TPU v7x, 512 devices: a whole 4x4x16 slice. The times are simulated.
512 devices in a mesh: sp: 32 (over z, core), tp: 16 (over y, x).
Axes of the slice: x: 4, y: 4, z: 16, core: 2. Of those that a mesh axis runs over, the one named last changes fastest.
Arguments:
- residual_in: bfloat16 [4096, 2048], P('sp', 'tp'), may hold values from -6 to 6
- query_wide: bfloat16 [4096, 2048], P('sp', 'tp'), may hold values from -6 to 6
- narrow_head_query: bfloat16 [4096, 1024], P('sp', 'tp'), may hold values from -6 to 6
- forget_wide: bfloat16 [4096, 2048], P('sp', 'tp'), may hold values from -6 to 6
- forget_narrow: bfloat16 [4096, 1024], P('sp', 'tp'), may hold values from -6 to 6
- room_wide: float32 [2048], P('tp'), as said below
- room_narrow: float32 [1024], P('tp'), as said below
- values: bfloat16 [4096, 2048], P('sp', 'tp'), may hold values from -6 to 6
- out_gate: bfloat16 [4096, 2048], P('sp', 'tp'), may hold values from -6 to 6
- head_gain: float32 [2048], P('tp'), may hold values from 0.1 to 1.9
- w_out: bfloat16 [2048, 2048], P(None, 'tp'), may hold values from -0.125 to 0.125
- norm_gain: float32 [2048], P('tp'), may hold values from 0.1 to 1.9
- route_ids: int32 [4096, 2], P('sp'), may hold values from 0 to 31, all different within a row; in each aligned block of 128 rows (0 to 127, 128 to 255, ...) at most 10 rows name the same one
- route_weight: float32 [4096, 2], P('sp'), may hold values from 0.25 to 1
- w_gate: bfloat16 [32, 2048, 4096], P('sp', None, 'tp'), may hold values from -0.125 to 0.125
- w_up: bfloat16 [32, 2048, 4096], P('sp', None, 'tp'), may hold values from -0.125 to 0.125
- w_down: bfloat16 [32, 4096, 2048], P('sp', 'tp'), may hold values from -0.09375 to 0.09375
Outputs:
- layer_out: bfloat16 [4096, 2048], P('sp', 'tp')
Inputs may be any that keep to these rules, and one draw needn't show every extreme that they name: `room_wide`: every value is positive and below 0.125. `room_narrow`: every value is positive and below 0.125. `route_ids`: each token names 2 different experts; among the 128 tokens of one index of sp no expert is named more than 10 times, and on some indices one is named exactly 10 times.
All inputs are finite; a program needn't handle non-finite values.
Results may differ from a plain program's by a relative error of at most 0.012.
Values may be sent and summed in bfloat16 or wider, within the bound.
A program may use at most 64 MiB of HBM per device.

v0:
```python
import functools

import jax
import jax.numpy as jnp
from jax import lax
from jax.sharding import Mesh
from jax.sharding import PartitionSpec as P

D = 2048
DKW = 128
DKN = 64
DV = 64
TOPK = 2
BLOCK = 64
SP = ("sp_0", "sp_1")
TP = ("tp_0", "tp_1")


EPS = 1e-06
TOP_PRECISION = lax.Precision.HIGHEST


def sent_together(arrays, axis, dim, along):
    widths = [a.shape[along] for a in arrays]
    both = jnp.concatenate(arrays, axis=along)
    result = lax.all_gather(both, axis, axis=dim, tiled=True)
    return tuple(jnp.split(result, [sum(widths[:k]) for k in range(1, len(widths))], axis=along))


def copy_for_each(value, axis):
    copies = jnp.broadcast_to(value, (lax.axis_size(axis), *value.shape))
    return lax.all_to_all(copies, axis, split_axis=0, concat_axis=0, tiled=True)


def in_order(parts, dim):
    parts = jnp.moveaxis(parts, 0, dim)
    shape = parts.shape
    return parts.reshape(*shape[:dim], shape[dim] * shape[dim + 1], *shape[dim + 2 :])


def gathered_copies(value, axis, dim):
    parts = copy_for_each(value, axis)
    return in_order(parts, dim)


def one_axis_at_a_time(value, axes):
    return functools.reduce(lax.psum, axes, value)


def split_up(value, dim, length):
    shape = value.shape
    parts = value.reshape(*shape[:dim], length, shape[dim] // length, *shape[dim + 1 :])
    return jnp.moveaxis(parts, dim, 0)


def turned_blocks(parts, axes, sequence):
    inside = parts.shape[1:]
    result = parts.reshape(*(lax.axis_size(a) for a in axes), *inside)
    for k in sequence:
        result = lax.all_to_all(result, axes[k], k, k, tiled=True)
    return result.reshape(-1, *inside)


def core_and_chips(value, groups, sequence, split_dim, concat_dim):
    length = lax.axis_size(groups[0]) * lax.axis_size(groups[1])
    parts = split_up(value, split_dim, length)
    return in_order(turned_blocks(parts, groups, sequence), concat_dim)


def sum_at_owner(value, axis, dim):
    parts = split_up(value, dim, lax.axis_size(axis))
    arrived = lax.all_to_all(parts, axis, split_axis=0, concat_axis=0, tiled=True)
    return arrived.astype(jnp.float32).sum(axis=0)


def run_blocks(queries, rates, contents, log_decay, block_len, initial):
    length, head_count, key_dim = queries.shape
    value_dim = contents.shape[-1]
    span_count = length // block_len

    def to_spans(tensor):
        return tensor.reshape(span_count, block_len, head_count, tensor.shape[-1]).transpose(
            0, 2, 1, 3
        )

    span_query = to_spans(queries)
    span_rate = to_spans(rates)
    span_value = to_spans(contents)
    inside = jnp.cumsum(to_spans(log_decay), axis=2)
    middle = inside[:, :, block_len // 2 - 1 : block_len // 2, :]
    ending = inside[:, :, block_len - 1 : block_len, :]
    near_query = span_query * jnp.exp(inside - middle)
    near_rate = span_rate * jnp.exp(middle - inside)
    far_query = span_query * jnp.exp(inside)
    far_rate = span_rate * jnp.exp(ending - inside)
    fading = jnp.exp(ending[:, :, 0, :])
    causal = jnp.tril(jnp.ones((block_len, block_len), jnp.float32))

    def advance(running_total, slice_pieces):
        scores = (
            jnp.einsum("htk,hsk->hts", slice_pieces[0], slice_pieces[1], precision=TOP_PRECISION)
            * causal
        )
        final_output = jnp.einsum("hts,hsv->htv", scores, slice_pieces[4], precision=TOP_PRECISION)
        final_output = final_output + jnp.einsum(
            "ncw,nws->ncs", slice_pieces[2], running_total, precision=TOP_PRECISION
        )
        running_total = slice_pieces[5][..., None] * running_total + jnp.einsum(
            "jlg,jlq->jgq", slice_pieces[3], slice_pieces[4], precision=TOP_PRECISION
        )
        return (running_total, final_output)

    final, outputs = lax.scan(
        advance, initial, (near_query, near_rate, far_query, far_rate, span_value, fading)
    )
    return (final, outputs.transpose(0, 2, 1, 3).reshape(length, head_count, value_dim))


def head_inputs(raw_query, raw_forget, room_vec, key_dim):
    length = raw_query.shape[0]
    activated = jax.nn.silu(raw_query.astype(jnp.float32)).reshape(length, -1, key_dim)
    in_rate = (room_vec * jax.nn.sigmoid(-raw_forget.astype(jnp.float32))).reshape(
        length, -1, key_dim
    )
    return (activated, in_rate, jnp.log1p(-in_rate))


def head_norm(outputs):
    return outputs * lax.rsqrt(jnp.mean(outputs * outputs, axis=-1, keepdims=True) + EPS)


def expert_apply(flat_rows, w_gate, w_up, w_down):
    gate_proj = jnp.dot(flat_rows, w_gate[0], preferred_element_type=jnp.float32)
    up_proj = jnp.dot(flat_rows, w_up[0], preferred_element_type=jnp.float32)
    hidden = (jax.nn.silu(gate_proj) * up_proj).astype(jnp.bfloat16)
    return jnp.dot(hidden, w_down[0], preferred_element_type=jnp.float32)


def body(
    residual_in,
    query_wide,
    narrow_head_query,
    forget_wide,
    forget_narrow,
    room_wide,
    room_narrow,
    values,
    out_gate,
    head_gain,
    w_out,
    norm_gain,
    route_ids,
    route_weight,
    w_gate,
    w_up,
    w_down,
):
    length = residual_in.shape[0]
    value_cols = values.astype(jnp.float32).reshape(length, -1, 2, DV)
    wide_query, wide_rate, wide_log = head_inputs(query_wide, forget_wide, room_wide, DKW)
    narrow_query, narrow_rate, narrow_log = head_inputs(
        narrow_head_query, forget_narrow, room_narrow, DKN
    )
    pair_count = wide_query.shape[1]
    wide_end, wide_out = run_blocks(
        wide_query,
        wide_rate,
        value_cols[:, :, 0],
        wide_log,
        BLOCK,
        jnp.zeros((pair_count, DKW, DV), jnp.float32),
    )
    narrow_end, narrow_out = run_blocks(
        narrow_query,
        narrow_rate,
        value_cols[:, :, 1],
        narrow_log,
        BLOCK,
        jnp.zeros((pair_count, DKN, DV), jnp.float32),
    )
    wide_sum = jnp.cumsum(wide_log, axis=0)
    narrow_sum = jnp.cumsum(narrow_log, axis=0)
    logs_all = sent_together((wide_sum[-1][None], narrow_sum[-1][None]), SP, 0, 2)
    position = lax.axis_index(SP)
    wide_upto = jnp.cumsum(logs_all[0], axis=0)
    narrow_upto = jnp.cumsum(logs_all[1], axis=0)
    wide_here = wide_upto[position] - logs_all[0][position]
    narrow_here = narrow_upto[position] - logs_all[1][position]
    pieces = sent_together((wide_end[None], narrow_end[None]), SP, 0, 2)
    tally_rows = pieces[0].shape[0]
    device_ids = jnp.arange(tally_rows, dtype=jnp.int32)
    before = (device_ids < position)[:, None, None]
    wide_gap = wide_here[None] - wide_upto
    narrow_gap = narrow_here[None] - narrow_upto
    wide_scale = jnp.where(before, jnp.exp(jnp.where(before, wide_gap, 0.0)), 0.0)
    narrow_scale = jnp.where(before, jnp.exp(jnp.where(before, narrow_gap, 0.0)), 0.0)
    wide_in = jnp.sum(wide_scale[..., None] * pieces[0], axis=0)
    narrow_in = jnp.sum(narrow_scale[..., None] * pieces[1], axis=0)
    wide_full = wide_out + jnp.einsum(
        "tpk,pkv->tpv", wide_query * jnp.exp(wide_sum), wide_in, precision=TOP_PRECISION
    )
    narrow_full = narrow_out + jnp.einsum(
        "tpk,pkv->tpv", narrow_query * jnp.exp(narrow_sum), narrow_in, precision=TOP_PRECISION
    )
    normed_heads = jnp.stack([head_norm(wide_full), head_norm(narrow_full)], axis=2).reshape(
        length, -1
    )
    mixed = (normed_heads * head_gain * jax.nn.silu(out_gate.astype(jnp.float32))).astype(
        jnp.bfloat16
    )
    projected = jnp.dot(gathered_copies(mixed, TP, 1), w_out, preferred_element_type=jnp.float32)
    residual_mid = (residual_in.astype(jnp.float32) + projected).astype(jnp.bfloat16)
    mid_float = residual_mid.astype(jnp.float32)
    squares = one_axis_at_a_time(jnp.sum(mid_float * mid_float, axis=1), TP)
    normed_cols = (mid_float * lax.rsqrt(squares / D + EPS)[:, None] * norm_gain).astype(
        jnp.bfloat16
    )
    experts = lax.axis_size(SP)
    capacity = (7 * TOPK * length + 6 * experts - 1) // (6 * experts)
    flat_ids = route_ids.reshape(-1)
    matches = (flat_ids[:, None] == jnp.arange(experts, dtype=jnp.int32)[None, :]).astype(jnp.int32)
    slot_rank = jnp.sum((jnp.cumsum(matches, axis=0) - matches) * matches, axis=1)
    positions = flat_ids * capacity + slot_rank
    owners = (
        jnp.full((experts * capacity,), length, jnp.int32)
        .at[positions]
        .set(jnp.arange(length * TOPK, dtype=jnp.int32) // TOPK)
    )
    outgoing = jnp.take(normed_cols, owners, axis=0, mode="fill", fill_value=0).reshape(
        experts, capacity, -1
    )
    whole_rows = gathered_copies(
        lax.all_to_all(outgoing, SP, split_axis=0, concat_axis=0, tiled=True), TP, 2
    )
    flat_rows = whole_rows.reshape(-1, whole_rows.shape[-1])
    partial_value = expert_apply(flat_rows, w_gate, w_up, w_down).reshape(
        whole_rows.shape[0], whole_rows.shape[1], -1
    )
    weights_flat = route_weight.reshape(-1, 1)
    handed_back = core_and_chips(
        partial_value.astype(jnp.bfloat16), ("sp_0", "sp_1"), (1, 0), 0, 0
    ).astype(partial_value.dtype)
    picked = jnp.take(handed_back.reshape(experts * capacity, -1), positions, axis=0)
    local_sum = jnp.sum((picked * weights_flat).reshape(length, TOPK, -1), axis=1)
    routed = sum_at_owner(local_sum.astype(jnp.bfloat16), TP, 1)
    return (mid_float + routed).astype(jnp.bfloat16)


def solution(mesh):
    torus = Mesh(mesh.devices.reshape(16, 2, 4, 4), ("sp_0", "sp_1", "tp_0", "tp_1"))
    placed = (
        P(SP, TP),
        P(SP, TP),
        P(SP, TP),
        P(SP, TP),
        P(SP, TP),
        P(TP),
        P(TP),
        P(SP, TP),
        P(SP, TP),
        P(TP),
        P(None, TP),
        P(TP),
        P(SP, None),
        P(SP, None),
        P(SP, None, TP),
        P(SP, None, TP),
        P(SP, TP, None),
    )
    return jax.shard_map(body, mesh=torus, in_specs=placed, out_specs=P(SP, TP), check_vma=False)
```

profile of v0, /device:TPU:1, one launch (start us, length us, event | category | flops | bytes accessed | tf_op | source)
XLA Modules:
  0.0 299.5 jit_solution(15607442959119795650)
XLA Ops:
  6.5 0.9 copy.184
  7.5 0.7 divide_multiply_fusion
  8.3 0.8 copy.188
  9.2 0.9 copy.179
  10.3 1.7 while.27
  10.3 0.2 convolution_multiply_fusion.5
  10.5 0.2 fusion.164
  10.6 0.2 fusion.165
  10.8 0.2 fusion.163
  11.1 0.2 convolution_multiply_fusion.5
  11.3 0.2 fusion.164
  11.5 0.2 fusion.165
  11.7 0.2 fusion.163
  12.4 1.7 while.26
  12.4 0.2 convolution_multiply_fusion.4
  12.6 0.2 fusion.152
  12.8 0.2 fusion.153
  13.0 0.2 fusion.151
  13.3 0.2 convolution_multiply_fusion.4
  13.5 0.2 fusion.152
  13.7 0.2 fusion.153
  13.9 0.2 fusion.151
  14.2 0.6 pad_maximum_fusion
  15.2 37.7 %all_gather.6 = f32[32,1,192]{2,1,0:T(1,128)S(1)} all-gather(f32[1,1,192]{2,1,0:T(1,128)S(1)} %pad_maximum_fusion.2), channel_id=1, replica_groups=mesh['sp_0'=16,'sp_1'=2,'tp_0'=4,'tp_1'=4] {'sp_0','sp_1'}, dimensions={0}, use_global_device_ids=true | all-gather | bytes 25344 | tf_op jit(solution)/shard_map/all_gather | solution.py:26
  53.7 0.6 reduce-window.6
  54.3 0.2 slice_reduce_fusion
  54.9 1.4 scatter_custom_fusion
  56.6 35.7 %all-gather.2.cloned.1.call-done = f32[32,1,192,64]{2,3,1,0:T(8,128)} async-done(((f32[1,1,192,64]{2,3,1,0:T(8,128)}), f32[32,1,192,64]{2,3,1,0:T(8,128)}) %all-gather.2.cloned.1.call-update) | async-done | bytes 1572880 | tf_op jit(solution)/shard_map/all_gather | solution.py:26
  92.2 1.3 fusion.73
  93.6 0.3 multiply_reduce_fusion.3
  93.8 1.4 fusion.72
  95.2 0.3 multiply_reduce_fusion.2
  95.8 0.9 broadcast_in_dim.116
  96.7 6.5 %all-to-all-start = ((bf16[16,128,128]{1,2,0:T(8,128)(2,1)}), bf16[16,128,128]{1,2,0:T(8,128)(2,1)S(1)}, u32[]{:S(2)}, u32[]{:S(2)}) async-start(bf16[16,128,128]{1,2,0:T(8,128)(2,1)} %broadcast_in_dim.116), calls=%async_computation | async-start | bytes 1048576 | tf_op jit(solution)/shard_map/all_to_all | solution.py:32
  103.3 10.7 %all-to-all-done = bf16[16,128,128]{1,2,0:T(8,128)(2,1)S(1)} async-done(((bf16[16,128,128]{1,2,0:T(8,128)(2,1)}), bf16[16,128,128]{1,2,0:T(8,128)(2,1)S(1)}, u32[]{:S(2)}, u32[]{:S(2)}) %all-to-all-start) | async-done | bytes 524320 | tf_op jit(solution)/shard_map/all_to_all | solution.py:32
  114.0 0.4 multiply_reduce_fusion.1
  114.4 6.6 %psum.14 = f32[128]{0:T(128)S(1)} all-reduce(f32[128]{0:T(128)S(1)} %get-tuple-element.351), channel_id=1, replica_groups=mesh['sp_0'=16,'sp_1'=2,'tp_0'=4,'tp_1'=4] {'tp_0'}, use_global_device_ids=true, to_apply=%region_19.20 | all-reduce | flops 128 | bytes 1024 | tf_op jit(solution)/shard_map/psum | solution.py:47
  120.9 7.1 %psum.15 = f32[128]{0:T(128)S(1)} all-reduce(f32[128]{0:T(128)S(1)} %psum.14), channel_id=1, replica_groups=mesh['sp_0'=16,'sp_1'=2,'tp_0'=4,'tp_1'=4] {'tp_1'}, use_global_device_ids=true, to_apply=%region_20.21 | all-reduce | flops 128 | bytes 1024 | tf_op jit(solution)/shard_map/psum | solution.py:47
  128.2 1.4 gather_fusion
  129.8 29.0 %all_to_all.30 = bf16[32,10,128]{2,1,0:T(8,128)(2,1)S(1)} all-to-all(bf16[32,10,128]{2,1,0:T(8,128)(2,1)S(1)} %broadcast_select_fusion), channel_id=1, replica_groups=mesh['sp_0'=16,'sp_1'=2,'tp_0'=4,'tp_1'=4] {'sp_0','sp_1'}, dimensions={0} | all-to-all | bytes 163840 | tf_op jit(solution)/shard_map/all_to_all | solution.py:233
  158.8 0.2 broadcast_in_dim.123
  159.1 20.7 %all_to_all.31 = bf16[16,32,10,128]{3,1,2,0:T(8,128)(2,1)S(1)} all-to-all(bf16[16,32,10,128]{3,1,2,0:T(8,128)(2,1)S(1)} %broadcast_in_dim.123), channel_id=1, replica_groups=mesh['sp_0'=16,'sp_1'=2,'tp_0'=4,'tp_1'=4] {'tp_0','tp_1'}, dimensions={0} | all-to-all | bytes 2621440 | tf_op jit(solution)/shard_map/all_to_all | solution.py:32
  179.8 0.8 copy.206
  180.7 0.4 copy-done.11
  181.0 0.5 fusion.58
  181.6 0.7 copy-done.12
  182.3 0.5 fusion.63
  182.9 0.5 convolution_convert_fusion
  183.4 1.7 reshape_reshape.8
  185.1 1.8 copy.208
  186.9 7.4 %all_to_all.32 = bf16[16,2,1,10,2048]{4,0,3,2,1:T(8,128)(2,1)S(1)} all-to-all(bf16[16,2,1,10,2048]{4,0,3,2,1:T(8,128)(2,1)S(1)} %copy.208), channel_id=1, replica_groups=mesh['sp_0'=16,'sp_1'=2,'tp_0'=4,'tp_1'=4] {'sp_1'}, dimensions={1} | all-to-all | bytes 2621440 | tf_op jit(solution)/shard_map/all_to_all | solution.py:60
  194.3 2.4 copy.209
  196.7 3.8 %all-to-all-start.4 = ((bf16[16,2,1,10,2048]{4,1,3,2,0:T(2,128)(2,1)}), bf16[16,2,1,10,2048]{4,1,3,2,0:T(2,128)(2,1)S(1)}, u32[]{:S(2)}, u32[]{:S(2)}) async-start(bf16[16,2,1,10,2048]{4,1,3,2,0:T(2,128)(2,1)} %copy.209), calls=%async_computation.4 | async-start | bytes 2621440 | tf_op jit(solution)/shard_map/all_to_all | solution.py:60
  201.1 57.7 %all-to-all-done.4 = bf16[16,2,1,10,2048]{4,1,3,2,0:T(2,128)(2,1)S(1)} async-done(((bf16[16,2,1,10,2048]{4,1,3,2,0:T(2,128)(2,1)}), bf16[16,2,1,10,2048]{4,1,3,2,0:T(2,128)(2,1)S(1)}, u32[]{:S(2)}, u32[]{:S(2)}) %all-to-all-start.4) | async-done | bytes 1310752 | tf_op jit(solution)/shard_map/all_to_all | solution.py:60
  258.7 0.8 copy_convert_fusion
  259.5 3.5 %copy.211 = f32[16,2,1,10,2048]{4,3,1,0,2:T(8,128)} copy(f32[16,2,1,10,2048]{4,0,3,2,1:T(8,128)S(1)} %copy_convert_fusion) | data formatting | bytes 5242880 | tf_op jit(solution)/shard_map/convert_element_type | solution.py:242
  263.0 4.5 %reshape.605 = f32[320,2048]{1,0:T(8,128)} reshape(f32[16,2,1,10,2048]{4,3,1,0,2:T(8,128)} %copy.211) | data formatting | bytes 5242880 | tf_op jit(solution)/shard_map/convert_element_type | solution.py:242
  267.5 4.1 %gather_fusion.1 = f32[256,2048]{1,0:T(8,128)S(1)} fusion(f32[320,2048]{1,0:T(8,128)} %reshape.605, s32[1024]{0:T(1024)S(1)} %pad_clamp_fusion), kind=kCustom, calls=%fused_computation.1 | custom fusion | bytes 4195328 | tf_op jit(solution)/shard_map/jit(_take)/gather | solution.py:243
  271.7 2.3 gather.15
  274.0 5.6 %multiply_reduce_fusion = bf16[128,2048]{1,0:T(8,128)(2,1)S(1)} fusion(f32[128,2,2048]{2,1,0:T(2,128)} %gather.15, pred[128,2]{1,0:T(8,128)(4,1)S(1)} %copy.202, f32[128,2]{1,0:T(8,128)S(1)} %copy.212), kind=kLoop, calls=%fused_computation.68 | loop fusion | flops 1310720 | bytes 2622720 | tf_op jit(solution)/shard_map/reduce_sum | solution.py:244
  279.6 0.3 copy.213
  279.8 0.3 copy.214
  280.1 11.6 %all_to_all.33 = bf16[16,128,128]{2,1,0:T(8,128)(2,1)S(1)} all-to-all(bf16[16,128,128]{2,1,0:T(8,128)(2,1)S(1)} %copy.214), channel_id=1, replica_groups=mesh['sp_0'=16,'sp_1'=2,'tp_0'=4,'tp_1'=4] {'tp_0','tp_1'}, dimensions={0} | all-to-all | bytes 1048576 | tf_op jit(solution)/shard_map/all_to_all | solution.py:72
  291.9 0.7 copy.216
  (105 shorter events, 4.1 us)
Async XLA Ops:
  6.5 176.3 %copy-start = (bf16[1,256,2048]{2,1,0:T(8,128)(2,1)S(1)}, bf16[1,256,2048]{2,1,0:T(8,128)(2,1)}, u32[]{:S(2)}) copy-start(bf16[1,256,2048]{2,1,0:T(8,128)(2,1)} %param.37) | copy-start | bytes 3145732
  6.5 85.7 %all-gather.2.cloned.1.call-start = ((), (), s32[]{:S(2)}) async-start(), calls=%async_computation.6 | async-start | bytes 2162688 | tf_op jit(solution)/shard_map/all_gather | solution.py:26
  10.2 1.8 copy-start.2
  10.2 1.8 copy-start.8
  10.2 2.0 copy-start.3
  12.4 40.6 %copy-start.6 = (s32[128,2]{0,1:T(2,128)S(1)}, s32[128,2]{0,1:T(2,128)}, u32[]{:S(2)}) copy-start(s32[128,2]{0,1:T(2,128)} %param.33) | copy-start | bytes 3076
  12.4 41.1 %copy-start.4 = (bf16[128,128]{1,0:T(8,128)(2,1)S(1)}, bf16[128,128]{1,0:T(8,128)(2,1)}, u32[]{:S(2)}) copy-start(bf16[128,128]{1,0:T(8,128)(2,1)} %param.21) | copy-start | bytes 98308
  93.5 2.1 copy-start.5
  93.5 2.1 copy-start.9
  95.2 18.8 %copy-start.1 = (bf16[2048,128]{1,0:T(8,128)(2,1)S(1)}, bf16[2048,128]{1,0:T(8,128)(2,1)}, u32[]{:S(2)}) copy-start(bf16[2048,128]{1,0:T(8,128)(2,1)} %param.31) | copy-start | bytes 1572868
  95.8 32.2 %copy-start.10 = (f32[128]{0:T(128)S(1)}, f32[128]{0:T(128)}, u32[]{:S(2)}) copy-start(f32[128]{0:T(128)} %param.32) | copy-start | bytes 1540
  96.7 17.3 %all-to-all-start = ((bf16[16,128,128]{1,2,0:T(8,128)(2,1)}), bf16[16,128,128]{1,2,0:T(8,128)(2,1)S(1)}, u32[]{:S(2)}, u32[]{:S(2)}) async-start(bf16[16,128,128]{1,2,0:T(8,128)(2,1)} %broadcast_in_dim.116), calls=%async_computation | async-start | bytes 1048576 | tf_op jit(solution)/shard_map/all_to_all | solution.py:32
  179.8 1.2 copy-start.11
  181.0 1.2 copy-start.12
  196.7 4.2 %copy-start.7 = (f32[128,2]{0,1:T(2,128)S(1)}, f32[128,2]{0,1:T(2,128)}, u32[]{:S(2)}) copy-start(f32[128,2]{0,1:T(2,128)} %param.34) | copy-start | bytes 3076
  196.7 62.0 %all-to-all-start.4 = ((bf16[16,2,1,10,2048]{4,1,3,2,0:T(2,128)(2,1)}), bf16[16,2,1,10,2048]{4,1,3,2,0:T(2,128)(2,1)S(1)}, u32[]{:S(2)}, u32[]{:S(2)}) async-start(bf16[16,2,1,10,2048]{4,1,3,2,0:T(2,128)(2,1)} %copy.209), calls=%async_computation.4 | async-start | bytes 2621440 | tf_op jit(solution)/shard_map/all_to_all | solution.py:60
Sparse Core Ops, SparseCore 0:
  14.9 77.2 all-gather.1
where the time goes:
time: 304 us; the launch traced here: 299 us
  blocking collectives  120 us (39%)
  waiting for transfers between devices  104 us (34%)
  local copies, waits for them, and re-layouts  32.9 us (11%)
  between operations  14 us (5%)
  other arithmetic  12.5 us (4%)
  starting transfers between devices  10.3 us (3%)
  matrix products  5.55 us (2%)
    all_to_all x1, waiting for transfers between devices, turned_blocks(): result = lax.all_to_all(result, axes[k], k, k, tiled=True)  57.7 us
    all_gather x1, blocking collectives, sent_together(): result = lax.all_gather(both, axis, axis=dim, tiled=True)  37.7 us
    all_gather x1, waiting for transfers between devices, sent_together(): result = lax.all_gather(both, axis, axis=dim, tiled=True)  35.7 us
    all_to_all x1, blocking collectives, body(): lax.all_to_all(outgoing, SP, split_axis=0, concat_axis=0, tiled=True)  29 us
    all_to_all x1, blocking collectives, copy_for_each(): return lax.all_to_all(copies, axis, split_axis=0, concat_axis=0, tiled=True)  20.7 us
    psum x2, blocking collectives, one_axis_at_a_time(): return functools.reduce(lax.psum, axes, value)  13.6 us
    all_to_all x1, blocking collectives, sum_at_owner(): lax.all_to_all(parts, axis, split_axis=0, concat_axis=0, tiled=True)  11.6 us
    all_to_all x1, waiting for transfers between devices, copy_for_each(): return lax.all_to_all(copies, axis, split_axis=0, concat_axis=0, tiled=True)  10.7 us
  transfers between devices with their start and end apart: 3, of which 3 were waited for; matrix products, arithmetic and copies ran while one was open for 2% of the time, Pallas kernels for 0%

commit v1 on v0

v1 whole, which is shorter than its diff:
```python
import functools

import jax
import jax.numpy as jnp
from jax import lax
from jax.experimental import pallas as pl
from jax.experimental.pallas import tpu as pltpu
from jax.sharding import PartitionSpec as P

D = 2048
DKW = 128
DKN = 64
DV = 64
EPS = 1e-06
CAP = 10
PADCAP = 16
F32 = jnp.float32
BF16 = jnp.bfloat16
TOP = lax.Precision.HIGHEST
MESH = pl.DeviceIdType.MESH


def dot(a, b, dims=((1,), (0,)), precision=None):
    return lax.dot_general(a, b, (dims, ((), ())), precision=precision, preferred_element_type=F32)


def silu(v):
    return v / (1.0 + jnp.exp(-v))


def iota(shape, dim):
    return lax.broadcasted_iota(jnp.int32, shape, dim)


def kernel(
    n_sp, n_tp, slots,
    res, qw, qn, fw, fn, room_w, room_n, val, gate_in, gain_h, w_out, gain_n, ids, rw, w_gate, w_up, w_down,
    out,
    wo_v, wg_v, wu_v, wd_v, w_sem,
    st, st_in, lg, lg_in, d2d_send, d2d_recv,
    t_src, t_buf, l_src, l_buf, t_send, t_recv, l_send, l_recv,
    x_src, x_in,
    mix, mix_send, mix_recv,
    gains, gain_send, gain_recv,
    disp_src, disp, disp_send, disp_recv,
    rows, rows_send, rows_recv,
    scat_src, scat, scat_send, scat_recv,
    ret_src, ret, ret_send, ret_recv,
    acc_g, acc_u,
):
    b = lax.axis_index("sp")
    p = lax.axis_index("tp")
    z = lax.div(b, 2)
    c = lax.rem(b, 2)
    chips = n_sp // 2
    partner = 2 * z + (1 - c)
    tokens = res.shape[0]
    padded = n_sp * PADCAP

    barrier = pltpu.get_barrier_semaphore()

    def greet_sp(i, _):
        pl.semaphore_signal(barrier, inc=1, device_id={"sp": lax.rem(b + i, n_sp)}, device_id_type=MESH)
        return 0

    def greet_tp(i, _):
        pl.semaphore_signal(barrier, inc=1, device_id={"tp": lax.rem(p + i, n_tp)}, device_id_type=MESH)
        return 0

    lax.fori_loop(1, n_sp, greet_sp, 0)
    lax.fori_loop(1, n_tp, greet_tp, 0)

    loads = [
        pltpu.make_async_copy(w_out, wo_v, w_sem.at[0]),
        pltpu.make_async_copy(w_gate.at[0], wg_v, w_sem.at[1]),
        pltpu.make_async_copy(w_up.at[0], wu_v, w_sem.at[2]),
        pltpu.make_async_copy(w_down.at[0], wd_v, w_sem.at[3]),
    ]
    for load in loads:
        load.start()

    def to_sp(src, dst, send, recv, who):
        return pltpu.make_async_remote_copy(src, dst, send, recv, device_id={"sp": who}, device_id_type=MESH)

    def to_tp(src, dst, send, recv, who):
        return pltpu.make_async_remote_copy(src, dst, send, recv, device_id={"tp": who}, device_id_type=MESH)

    low = (iota((tokens, tokens), 0) >= iota((tokens, tokens), 1)).astype(F32)

    def head(q_ref, f_ref, room_ref):
        q = silu(q_ref[...].astype(F32))
        rate = room_ref[...] / (1.0 + jnp.exp(f_ref[...].astype(F32)))
        cum = dot(low, jnp.log1p(-rate), precision=TOP)
        mid = cum[tokens // 2 - 1 : tokens // 2, :]
        end = cum[tokens - 1 : tokens, :]
        return q * jnp.exp(cum - mid), rate * jnp.exp(mid - cum), q * jnp.exp(cum), rate * jnp.exp(end - cum), end

    near_qw, near_rw, far_qw, far_rw, end_w = head(qw, fw, room_w)
    near_qn, near_rn, far_qn, far_rn, end_n = head(qn, fn, room_n)
    v = val[...].astype(F32)
    v_t = v.T
    s_w = dot(v_t[:DV], far_rw, precision=TOP)
    s_n = dot(v_t[DV:], far_rn, precision=TOP)
    s_n = jnp.concatenate([s_n[: DV // 2], s_n[DV // 2 :]], axis=1)
    st[0] = s_w[:48]
    st[1] = jnp.concatenate([s_w[48:], s_n], axis=0)
    lg[...] = jnp.concatenate([end_w, jnp.concatenate([end_n, end_n], axis=1)], axis=0)

    pl.semaphore_wait(barrier, n_sp + n_tp - 2)

    st_copy = to_sp(st.at[1 - c], st_in, d2d_send.at[0], d2d_recv.at[0], partner)
    lg_copy = to_sp(lg, lg_in, d2d_send.at[1], d2d_recv.at[1], partner)
    st_copy.start()
    lg_copy.start()

    gains[p] = jnp.broadcast_to(gain_n[...], gains.shape[1:])

    def send_gain(i, _):
        who = lax.rem(p + i, n_tp)
        to_tp(gains.at[p], gains.at[p], gain_send.at[i], gain_recv.at[p], who).start()
        return 0

    lax.fori_loop(1, n_tp, send_gain, 0)

    own_rows = iota((48, 128), 0) + 48 * c < DV

    def decay(logs):
        return jnp.exp(jnp.where(own_rows, logs[0:1], logs[1:2]))

    st_copy.wait_recv()
    lg_copy.wait_recv()
    own, other = st[c], st_in[...]
    own_log, other_log = lg[...], lg_in[...]
    first = c == 0
    even, odd = jnp.where(first, own, other), jnp.where(first, other, own)
    even_log = jnp.where(first, own_log, other_log)
    odd_log = jnp.where(first, other_log, own_log)
    t_src[...] = (decay(odd_log) * even + odd).astype(BF16)
    l_src[...] = even_log + odd_log

    def t_copy(i):
        return to_sp(t_src, t_buf.at[z], t_send.at[i], t_recv.at[z], 2 * i + c)

    def l_copy(i):
        return to_sp(l_src, l_buf.at[z], l_send.at[i], l_recv.at[z], 2 * i + c)

    def send_state(i, _):
        l_copy(i).start()
        t_copy(i).start()
        return 0

    lax.fori_loop(z + 1, chips, send_state, 0)

    def inside(near_q, near_r, content):
        scores = dot(near_q, near_r, ((1,), (1,)), precision=TOP) * low
        return dot(scores, content, precision=TOP)

    out_w = inside(near_qw, near_rw, v[:, :DV])
    out_n = inside(near_qn, near_rn, v[:, DV:])
    gated = gain_h[...] * silu(gate_in[...].astype(F32))

    lane = iota((tokens, n_sp), 1)
    hit0 = (lane == ids[:, 0:1]).astype(F32)
    hit1 = (lane == ids[:, 1:2]).astype(F32)
    strict = (iota((tokens, tokens), 0) > iota((tokens, tokens), 1)).astype(F32)
    taken = dot(strict.astype(BF16), (hit0 + hit1).astype(BF16))
    rank0 = jnp.sum(taken * hit0, axis=1, keepdims=True)
    rank1 = jnp.sum((taken + hit0) * hit1, axis=1, keepdims=True)
    pos0 = ids[:, 0:1].astype(F32) * PADCAP + rank0
    pos1 = ids[:, 1:2].astype(F32) * PADCAP + rank1
    row0 = jnp.broadcast_to(pos0, (tokens, tokens)).T[0:1]
    row1 = jnp.broadcast_to(pos1, (tokens, tokens)).T[0:1]
    slot = iota((padded, tokens), 0).astype(F32)
    pick = ((slot == row0) | (slot == row1)).astype(BF16)
    column = iota((tokens, padded), 1).astype(F32)
    weigh = jnp.where(column == pos0, rw[:, 0:1], 0.0) + jnp.where(column == pos1, rw[:, 1:2], 0.0)
    weigh_hi = weigh.astype(BF16)
    weigh_lo = (weigh - weigh_hi.astype(F32)).astype(BF16)
    filled = iota((slots, padded), 0).astype(F32)
    filled = filled + (PADCAP - CAP) * jnp.floor((filled + 0.5) * (1.0 / CAP))
    squeeze = (filled == iota((slots, padded), 1).astype(F32)).astype(BF16)
    spread = iota((padded, slots), 1).astype(F32)
    spread = spread + (PADCAP - CAP) * jnp.floor((spread + 0.5) * (1.0 / CAP))
    spread = (spread == iota((padded, slots), 0).astype(F32)).astype(BF16)

    def fold(i, carry):
        to_sp(l_src, l_buf.at[i], l_send.at[i], l_recv.at[i], partner).wait_recv()
        to_sp(t_src, t_buf.at[i], t_send.at[i], t_recv.at[i], partner).wait_recv()
        return decay(l_buf[i]) * carry + t_buf[i].astype(F32)

    in_even = lax.fori_loop(0, z, fold, jnp.zeros((48, 128), F32))
    in_odd = decay(even_log) * in_even + even
    x_src[...] = jnp.where(first, in_odd, in_even)
    x_copy = to_sp(x_src, x_in, d2d_send.at[2], d2d_recv.at[2], partner)
    x_copy.start()
    x_copy.wait_recv()
    half_own, half_other = jnp.where(first, in_even, in_odd), x_in[...]
    half0, half1 = jnp.where(first, half_own, half_other), jnp.where(first, half_other, half_own)
    in_w = jnp.concatenate([half0, half1[:16]], axis=0)
    in_n = half1[16:]
    in_n = jnp.concatenate([in_n[:, :DKN], in_n[:, DKN:]], axis=0)
    out_w = out_w + dot(far_qw, in_w, ((1,), (1,)), precision=TOP)
    out_n = out_n + dot(far_qn, in_n, ((1,), (1,)), precision=TOP)

    def normed(o):
        return o * lax.rsqrt(jnp.mean(o * o, axis=1, keepdims=True) + EPS)

    mix[p] = (jnp.concatenate([normed(out_w), normed(out_n)], axis=1) * gated).astype(BF16)

    def send_mix(i, _):
        to_tp(mix.at[p], mix.at[p], mix_send.at[i], mix_recv.at[p], lax.rem(p + i, n_tp)).start()
        return 0

    lax.fori_loop(1, n_tp, send_mix, 0)
    loads[0].wait()

    def w_out_rows(s):
        return wo_v[pl.ds(pl.multiple_of(s * 128, 128), 128), :]

    def project(i, total):
        s = lax.rem(p + n_tp - i, n_tp)
        to_tp(mix.at[s], mix.at[s], mix_send.at[i], mix_recv.at[s], s).wait_recv()
        return total + dot(mix[s], w_out_rows(s))

    projected = lax.fori_loop(1, n_tp, project, dot(mix[p], w_out_rows(p)))
    mid = (res[...].astype(F32) + projected).astype(BF16)

    packed = dot(pick, mid).astype(BF16)
    disp_src[...] = packed.reshape(n_sp, PADCAP, 128)
    disp[b] = disp_src[b]

    def send_rows(i, _):
        who = lax.rem(b + i, n_sp)
        to_sp(disp_src.at[who], disp.at[b], disp_send.at[i], disp_recv.at[b], who).start()
        return 0

    lax.fori_loop(1, n_sp, send_rows, 0)

    def have_rows(i, _):
        s = lax.rem(b + i, n_sp)
        to_sp(disp_src.at[s], disp.at[s], disp_send.at[i], disp_recv.at[s], s).wait_recv()
        return 0

    lax.fori_loop(1, n_sp, have_rows, 0)
    rows[p] = dot(squeeze, disp[...].reshape(padded, 128)).astype(BF16)

    def spread_rows(i, _):
        to_tp(rows.at[p], rows.at[p], rows_send.at[i], rows_recv.at[p], lax.rem(p + i, n_tp)).start()
        return 0

    lax.fori_loop(1, n_tp, spread_rows, 0)

    def have_gain(i, _):
        s = lax.rem(p + i, n_tp)
        to_tp(gains.at[s], gains.at[s], gain_send.at[i], gain_recv.at[s], s).wait_recv()
        return 0

    lax.fori_loop(1, n_tp, have_gain, 0)
    for load in loads[1:]:
        load.wait()
    acc_g[...] = jnp.zeros_like(acc_g)
    acc_u[...] = jnp.zeros_like(acc_u)

    def gate_up(s, squares):
        x = rows[s].astype(F32)
        y = (x * gains[s][0:1]).astype(BF16)
        at = pl.ds(pl.multiple_of(s * 128, 128), 128)
        acc_g[...] += dot(y, wg_v[at, :])
        acc_u[...] += dot(y, wu_v[at, :])
        return squares + x * x

    def gate_up_from(i, squares):
        s = lax.rem(p + n_tp - i, n_tp)
        to_tp(rows.at[s], rows.at[s], rows_send.at[i], rows_recv.at[s], s).wait_recv()
        return gate_up(s, squares)

    squares = lax.fori_loop(1, n_tp, gate_up_from, gate_up(p, jnp.zeros((slots, 128), F32)))
    scale = lax.rsqrt(jnp.sum(squares, axis=1, keepdims=True) * (1.0 / D) + EPS)
    hidden = (silu(acc_g[...] * scale) * (acc_u[...] * scale)).astype(BF16)

    def down(j):
        return dot(hidden, wd_v[:, pl.ds(pl.multiple_of(j * 128, 128), 128)])

    def send_part(i, _):
        who = lax.rem(p + i, n_tp)
        scat_src[who] = down(who).astype(BF16)
        to_tp(scat_src.at[who], scat.at[p], scat_send.at[i], scat_recv.at[p], who).start()
        return 0

    lax.fori_loop(1, n_tp, send_part, 0)

    def add_part(i, total):
        s = lax.rem(p + n_tp - i, n_tp)
        to_tp(scat_src.at[s], scat.at[s], scat_send.at[i], scat_recv.at[s], s).wait_recv()
        return total + scat[s].astype(F32)

    total = lax.fori_loop(1, n_tp, add_part, down(p)).astype(BF16)

    ret_src[...] = dot(spread, total).astype(BF16).reshape(n_sp, PADCAP, 128)
    ret[b] = ret_src[b]

    def send_back(i, _):
        who = lax.rem(b + i, n_sp)
        to_sp(ret_src.at[who], ret.at[b], ret_send.at[i], ret_recv.at[b], who).start()
        return 0

    lax.fori_loop(1, n_sp, send_back, 0)

    def have_back(i, _):
        s = lax.rem(b + i, n_sp)
        to_sp(ret_src.at[s], ret.at[s], ret_send.at[i], ret_recv.at[s], s).wait_recv()
        return 0

    lax.fori_loop(1, n_sp, have_back, 0)
    back = ret[...].reshape(padded, 128)
    moe = dot(weigh_hi, back) + dot(weigh_lo, back)
    out[...] = (mid.astype(F32) + moe).astype(BF16)

    st_copy.wait_send()
    lg_copy.wait_send()
    x_copy.wait_send()

    def state_gone(i, _):
        t_copy(i).wait_send()
        l_copy(i).wait_send()
        return 0

    lax.fori_loop(z + 1, chips, state_gone, 0)

    def tp_gone(i, _):
        who = lax.rem(p + i, n_tp)
        to_tp(gains.at[p], gains.at[p], gain_send.at[i], gain_recv.at[p], who).wait_send()
        to_tp(mix.at[p], mix.at[p], mix_send.at[i], mix_recv.at[p], who).wait_send()
        to_tp(rows.at[p], rows.at[p], rows_send.at[i], rows_recv.at[p], who).wait_send()
        to_tp(scat_src.at[who], scat.at[p], scat_send.at[i], scat_recv.at[p], who).wait_send()
        return 0

    lax.fori_loop(1, n_tp, tp_gone, 0)

    def sp_gone(i, _):
        who = lax.rem(b + i, n_sp)
        to_sp(disp_src.at[who], disp.at[b], disp_send.at[i], disp_recv.at[b], who).wait_send()
        to_sp(ret_src.at[who], ret.at[b], ret_send.at[i], ret_recv.at[b], who).wait_send()
        return 0

    lax.fori_loop(1, n_sp, sp_gone, 0)


def body(n_sp, n_tp, *args):
    (res, qw, qn, fw, fn, room_w, room_n, val, gate_in, gain_h, w_out, gain_n, ids, rw, w_gate, w_up, w_down) = args
    tokens = res.shape[0]
    hidden = w_gate.shape[2]
    chips = n_sp // 2
    slots = n_sp * CAP
    row = lambda a: a.reshape(1, -1)
    vmem = pl.BlockSpec(memory_space=pltpu.VMEM)
    hbm = pl.BlockSpec(memory_space=pl.ANY)
    dma = pltpu.SemaphoreType.DMA
    V = pltpu.VMEM
    scratch = [
        V((D, 128), BF16), V((D, hidden), BF16), V((D, hidden), BF16), V((hidden, D), BF16), dma((4,)),
        V((2, 48, 128), F32), V((48, 128), F32), V((2, 128), F32), V((2, 128), F32), dma((3,)), dma((3,)),
        V((48, 128), BF16), V((chips, 48, 128), BF16), V((2, 128), F32), V((chips, 2, 128), F32),
        dma((chips,)), dma((chips,)), dma((chips,)), dma((chips,)),
        V((48, 128), F32), V((48, 128), F32),
        V((n_tp, tokens, 128), BF16), dma((n_tp,)), dma((n_tp,)),
        V((n_tp, 8, 128), F32), dma((n_tp,)), dma((n_tp,)),
        V((n_sp, PADCAP, 128), BF16), V((n_sp, PADCAP, 128), BF16), dma((n_sp,)), dma((n_sp,)),
        V((n_tp, slots, 128), BF16), dma((n_tp,)), dma((n_tp,)),
        V((n_tp, slots, 128), BF16), V((n_tp, slots, 128), BF16), dma((n_tp,)), dma((n_tp,)),
        V((n_sp, PADCAP, 128), BF16), V((n_sp, PADCAP, 128), BF16), dma((n_sp,)), dma((n_sp,)),
        V((slots, hidden), F32), V((slots, hidden), F32),
    ]
    return pl.pallas_call(
        functools.partial(kernel, n_sp, n_tp, slots),
        out_shape=jax.ShapeDtypeStruct((tokens, 128), BF16),
        in_specs=[vmem] * 10 + [hbm] + [vmem] * 3 + [hbm] * 3,
        out_specs=vmem,
        scratch_shapes=scratch,
        compiler_params=pltpu.CompilerParams(
            collective_id=0, has_side_effects=True, vmem_limit_bytes=48 * 1024 * 1024
        ),
    )(res, qw, qn, fw, fn, row(room_w), row(room_n), val, gate_in, row(gain_h), w_out, row(gain_n), ids, rw, w_gate, w_up, w_down)


def solution(mesh):
    both = P("sp", "tp")
    placed = (
        both, both, both, both, both, P("tp"), P("tp"), both, both, P("tp"), P(None, "tp"), P("tp"),
        P("sp", None), P("sp", None), P("sp", None, "tp"), P("sp", None, "tp"), P("sp", "tp", None),
    )
    fn = functools.partial(body, mesh.shape["sp"], mesh.shape["tp"])
    return jax.shard_map(fn, mesh=mesh, in_specs=placed, out_specs=both, check_vma=False)
```

time: 304 us -> 112 us (0.37); the launches traced: 299 us -> 112 us
  blocking collectives: 120 us -> 0 us
  Pallas kernels: 0 us -> 104 us
  waiting for transfers between devices: 104 us -> 0 us
  local copies, waits for them, and re-layouts: 32.9 us -> 7.7 us
  between operations: 14 us -> 0.1 us
  other arithmetic: 12.5 us -> 0 us
  starting transfers between devices: 10.3 us -> 0 us
  matrix products: 5.55 us -> 0 us
    pallas_call x0 -> x1, Pallas kernels: none -> 104 us  [body(): pl.pallas_call(functools.partial(kernel, n_sp, n_tp, slots), out_shape=ja...]
    all_to_all x4 -> x0, blocking collectives: 68.7 us -> none  [the longest x1 29 us: body(): lax.all_to_all(outgoing, SP, split_axis=0, concat_axis=0, tiled=True)]
    all_to_all x2 -> x0, waiting for transfers between devices: 68.3 us -> none  [the longest x1 57.7 us: turned_blocks(): result = lax.all_to_all(result, axes[k], k, k, tiled=True)]
    all_gather x1 -> x0, blocking collectives: 37.7 us -> none  [sent_together(): result = lax.all_gather(both, axis, axis=dim, tiled=True)]
    all_gather x1 -> x0, waiting for transfers between devices: 35.7 us -> none  [sent_together(): result = lax.all_gather(both, axis, axis=dim, tiled=True)]
    psum x2 -> x0, blocking collectives: 13.6 us -> none  [one_axis_at_a_time(): return functools.reduce(lax.psum, axes, value)]
    all_to_all x2 -> x0, starting transfers between devices: 10.3 us -> none  [the longest x1 6.48 us: copy_for_each(): return lax.all_to_all(copies, axis, split_axis=0, concat_axis=0, tiled=True)]
    convert_element_type x6 -> x0, local copies, waits for them, and re-layouts: 9.26 us -> none  [the longest x2 8.04 us: body(): handed_back = core_and_chips(partial_value.astype(jnp.bfloat16), ('sp_0',...]
  transfers between devices with their start and end apart: 3 -> 0, of which waited for: 3 -> 0; matrix products, arithmetic and copies ran while one was open for 2% -> 0% of each run, Pallas kernels for 0% -> 0%
where the time goes in v1:
time: 112 us
  Pallas kernels  104 us (93%)
  local copies, waits for them, and re-layouts  7.7 us (7%)
    pallas_call x1, Pallas kernels, body(): pl.pallas_call(functools.partial(kernel, n_sp, n_tp, slots), out_shape=ja...  104 us
    unnamed x37, local copies, waits for them, and re-layouts  7.7 us

profile of v1, /device:TPU:1, one launch (start us, length us, event | category | flops | bytes accessed | tf_op | source)
XLA Modules:
  0.0 111.8 jit_solution(13818336846183576422)
XLA Ops:
  0.0 0.0 copy-start.13
  0.0 0.8 copy.18.qn
  0.8 0.0 copy-done.13
  0.9 0.0 copy-start.14
  0.9 0.0 copy-start.15
  0.9 0.0 copy-start.8
  0.9 0.1 copy.19.fn
  1.0 0.5 copy-done.14
  1.5 0.0 copy-start.6
  1.5 0.0 copy-start.7
  1.5 0.0 copy-start.11
  1.5 0.0 copy-start.12
  1.5 0.1 copy.20.ids
  1.7 0.0 copy-done.15
  1.7 0.0 copy-start.4
  1.7 0.0 copy-start.5
  1.7 0.0 copy-start.9
  1.7 0.0 copy-start.10
  1.7 0.1 copy.21.rw
  1.8 0.0 copy-done.8
  1.8 0.5 copy-done.6
  2.3 0.0 copy-done.7
  2.3 0.0 copy-done.11
  2.3 0.0 copy-done.12
  2.3 0.1 copy-done.4
  2.4 0.0 copy-done.5
  2.4 0.0 copy-done.9
  2.5 0.0 copy-done.10
  2.5 0.0 copy-start
  2.5 1.2 %copy-done = bf16[1,2048,256]{2,1,0:T(8,128)(2,1)S(1)} copy-done((bf16[1,2048,256]{2,1,0:T(8,128)(2,1)S(1)}, bf16[1,2048,256]{2,1,0:T(8,128)(2,1)}, u32[]{:S(2)}) %copy-start) | copy-done | bytes 1048600
  3.7 0.0 copy-start.1
  3.7 1.2 %copy-done.1 = bf16[1,2048,256]{2,1,0:T(8,128)(2,1)S(1)} copy-done((bf16[1,2048,256]{2,1,0:T(8,128)(2,1)S(1)}, bf16[1,2048,256]{2,1,0:T(8,128)(2,1)}, u32[]{:S(2)}) %copy-start.1) | copy-done | bytes 1048600
  4.9 0.0 copy-start.2
  4.9 1.2 %copy-done.2 = bf16[1,256,2048]{2,1,0:T(8,128)(2,1)S(1)} copy-done((bf16[1,256,2048]{2,1,0:T(8,128)(2,1)S(1)}, bf16[1,256,2048]{2,1,0:T(8,128)(2,1)}, u32[]{:S(2)}) %copy-start.2) | copy-done | bytes 1048600
  6.1 0.0 copy-start.3
  6.1 1.0 copy-done.3
  7.2 104.0 %shard_map.163 = bf16[128,128]{1,0:T(8,128)(2,1)S(1)} custom-call(bf16[128,128]{1,0:T(8,128)(2,1)S(1)} %copy-done.4, bf16[128,128]{1,0:T(8,128)(2,1)S(1)} %copy-done.5, bf16[128,64]{1,0:T(8,128)(2,1)S(1)} %copy.18.qn, bf16[128,128]{1,0:T(8,128)(2,1)S(1)} %copy-done.6, bf16[128,64]{1,0:T(8,128)(2,1)S(1)} %copy.19.fn, f32[1,128]{1,0:T(1,128)S(1)} %bitcast.4, ...), custom_call_target="tpu_custom_call" | custom-call | tf_op jit(solution)/shard_map/pallas_call | solution.py:374
  111.1 0.6 copy.23
Async XLA Ops:
  0.0 0.8 copy-start.13
  0.9 0.7 copy-start.14
  0.9 0.8 copy-start.15
  0.9 1.0 copy-start.8
  1.5 0.8 copy-start.6
  1.5 0.8 copy-start.7
  1.5 0.8 copy-start.11
  1.5 0.8 copy-start.12
  1.7 0.8 copy-start.4
  1.7 0.8 copy-start.5
  1.7 0.8 copy-start.9
  1.7 0.8 copy-start.10
  2.5 1.2 %copy-start = (bf16[1,2048,256]{2,1,0:T(8,128)(2,1)S(1)}, bf16[1,2048,256]{2,1,0:T(8,128)(2,1)}, u32[]{:S(2)}) copy-start(bf16[1,2048,256]{2,1,0:T(8,128)(2,1)} %w_gate.1) | copy-start | bytes 3145732
  3.7 1.2 %copy-start.1 = (bf16[1,2048,256]{2,1,0:T(8,128)(2,1)S(1)}, bf16[1,2048,256]{2,1,0:T(8,128)(2,1)}, u32[]{:S(2)}) copy-start(bf16[1,2048,256]{2,1,0:T(8,128)(2,1)} %w_up.1) | copy-start | bytes 3145732
  4.9 1.2 %copy-start.2 = (bf16[1,256,2048]{2,1,0:T(8,128)(2,1)S(1)}, bf16[1,256,2048]{2,1,0:T(8,128)(2,1)}, u32[]{:S(2)}) copy-start(bf16[1,256,2048]{2,1,0:T(8,128)(2,1)} %w_down.1) | copy-start | bytes 3145732
  6.1 1.0 copy-start.3

commit v2 on v1

v2 whole, which is shorter than its diff:
```python
import functools

import jax
import jax.numpy as jnp
from jax import lax
from jax.experimental import pallas as pl
from jax.experimental.pallas import tpu as pltpu
from jax.sharding import PartitionSpec as P

D = 2048
DKW = 128
DKN = 64
DV = 64
EPS = 1e-06
CAP = 10
PADCAP = 16
NODE = 4
PART = (DV + DV // 2) // NODE
F32 = jnp.float32
BF16 = jnp.bfloat16
TOP = lax.Precision.HIGHEST
MESH = pl.DeviceIdType.MESH


PROFILE = False
scope = []


def mark(name=None):
    if PROFILE:
        while scope:
            scope.pop().__exit__(None, None, None)
        if name:
            scope.append(jax.named_scope(name))
            scope[-1].__enter__()


def dot(a, b, dims=((1,), (0,)), precision=None):
    return lax.dot_general(a, b, (dims, ((), ())), precision=precision, preferred_element_type=F32)


def silu(v):
    return v / (1.0 + jnp.exp(-v))


def iota(shape, dim):
    return lax.broadcasted_iota(jnp.int32, shape, dim)


def kernel(
    n_sp, n_tp, slots,
    res_h, qw_h, qn_h, fw_h, fn_h, room_w_h, room_n_h, val_h, gate_h, gain_h_h, w_out, gain_n_h, ids_h, rw_h,
    w_gate, w_up, w_down,
    out,
    res, qw, qn, fw, fn, room_w, room_n, val, gate_in, gain_h, gain_n, ids, rw, in_sem,
    wo_v, wgu, wd_v, w_sem,
    st, st_in, st_send, st_recv, lg, lg_send, lg_recv,
    t_src, t_buf, l_src, l_buf, t_send, t_recv, l_send, l_recv,
    x_src, x_in, x_send, x_recv,
    mix, mix_send, mix_recv,
    gains, gain_send, gain_recv,
    disp_src, disp, disp_send, disp_recv,
    rows, rows_send, rows_recv,
    heavy_src, heavy, heavy_send, heavy_recv,
    light_src, light, light_send, light_recv,
    keep, line,
    ret_src, ret, ret_send, ret_recv,
    acc, squares,
):
    b = lax.axis_index("sp")
    p = lax.axis_index("tp")
    nodes = n_sp // NODE
    node, q = lax.div(b, NODE), lax.rem(b, NODE)
    tokens = res.shape[0]
    padded = n_sp * PADCAP

    small = (
        (qw_h, qw), (fw_h, fw), (qn_h, qn), (fn_h, fn), (room_w_h, room_w), (room_n_h, room_n), (val_h, val),
        (gate_h, gate_in), (gain_h_h, gain_h), (gain_n_h, gain_n), (ids_h, ids), (rw_h, rw), (res_h, res),
    )
    small = [pltpu.make_async_copy(src, dst, in_sem.at[k]) for k, (src, dst) in enumerate(small)]
    hidden_units = w_down.shape[1]
    loads = [
        pltpu.make_async_copy(w_out, wo_v, w_sem.at[0]),
        pltpu.make_async_copy(w_gate.at[0], wgu.at[:, pl.ds(0, hidden_units)], w_sem.at[1]),
        pltpu.make_async_copy(w_up.at[0], wgu.at[:, pl.ds(hidden_units, hidden_units)], w_sem.at[2]),
    ]
    for k in range(n_tp):
        loads.append(pltpu.make_async_copy(w_down.at[0, :, pl.ds(128 * k, 128)], wd_v.at[k], w_sem.at[3 + k]))
    for load in small:
        load.start()
    disp[...] = jnp.zeros_like(disp)
    ret[...] = jnp.zeros_like(ret)

    barrier = pltpu.get_barrier_semaphore()

    def greet_sp(i, _):
        pl.semaphore_signal(barrier, inc=1, device_id={"sp": lax.rem(b + i, n_sp)}, device_id_type=MESH)
        return 0

    def greet_tp(i, _):
        pl.semaphore_signal(barrier, inc=1, device_id={"tp": lax.rem(p + i, n_tp)}, device_id_type=MESH)
        return 0

    lax.fori_loop(1, n_sp, greet_sp, 0)
    lax.fori_loop(1, n_tp, greet_tp, 0)
    for load in loads:
        load.start()
    for load in small:
        load.wait()

    def to_sp(src, dst, send, recv, who):
        return pltpu.make_async_remote_copy(src, dst, send, recv, device_id={"sp": who}, device_id_type=MESH)

    def to_tp(src, dst, send, recv, who):
        return pltpu.make_async_remote_copy(src, dst, send, recv, device_id={"tp": who}, device_id_type=MESH)

    mark("local")
    low = (iota((tokens, tokens), 0) >= iota((tokens, tokens), 1)).astype(F32)

    def head(q, f, room_ref):
        q = silu(q)
        rate = room_ref[...] / (1.0 + jnp.exp(f))
        cum = dot(low, jnp.log1p(-rate), precision=TOP)
        mid = cum[tokens // 2 - 1 : tokens // 2, :]
        end = cum[tokens - 1 : tokens, :]
        return q * jnp.exp(cum - mid), rate * jnp.exp(mid - cum), q * jnp.exp(cum), rate * jnp.exp(end - cum), end

    near_qw, near_rw, far_qw, far_rw, end_w = head(qw[...].astype(F32), fw[...].astype(F32), room_w)
    near_qn, near_rn, far_qn, far_rn, end_n = head(qn[...].astype(F32).T, fn[...].astype(F32).T, room_n)
    v = val[...].astype(F32)
    v_t = v.T
    s_w = dot(v_t[:DV], far_rw, precision=TOP)
    s_n = dot(v_t[DV:], far_rn, precision=TOP)
    s_n = jnp.concatenate([s_n[: DV // 2], s_n[DV // 2 :]], axis=1)
    states = jnp.concatenate([s_w, s_n], axis=0)
    for j in range(NODE):
        st[j] = states[j * PART : (j + 1) * PART]
    lg[q] = jnp.concatenate([end_w, jnp.concatenate([end_n, end_n], axis=1)], axis=0)

    mark("barrier")
    pl.semaphore_wait(barrier, n_sp + n_tp - 2)

    mark("d2d")
    def mate(i):
        return lax.rem(q + i, NODE)

    def st_copy(i, who, slot):
        return to_sp(st.at[who], st_in.at[slot], st_send.at[i], st_recv.at[slot], NODE * node + who)

    def lg_copy(i, who, slot):
        return to_sp(lg.at[slot], lg.at[slot], lg_send.at[i], lg_recv.at[slot], NODE * node + who)

    def x_copy(i, who, slot):
        return to_sp(x_src.at[who], x_in.at[slot], x_send.at[i], x_recv.at[slot], NODE * node + who)

    for i in range(1, NODE):
        lg_copy(i, mate(i), q).start()
        st_copy(i, mate(i), q).start()
    st_in[q] = st[q]

    gains[p] = jnp.broadcast_to(gain_n[...], gains.shape[1:])

    def send_gain(i, _):
        who = lax.rem(p + i, n_tp)
        to_tp(gains.at[p], gains.at[p], gain_send.at[i], gain_recv.at[p], who).start()
        return 0

    lax.fori_loop(1, n_tp, send_gain, 0)

    own_rows = iota((PART, 128), 0) + PART * q < DV

    def decay(logs):
        return jnp.exp(jnp.where(own_rows, logs[0:1], logs[1:2]))

    mark("d2dwait")
    for i in range(1, NODE):
        lg_copy(i, mate(i), mate(i)).wait_recv()
        st_copy(i, mate(i), mate(i)).wait_recv()
    decays = [decay(lg[j]) for j in range(NODE)]
    whole = st_in[0]
    for j in range(1, NODE):
        whole = decays[j] * whole + st_in[j]
    t_src[...] = whole.astype(BF16)
    l_src[...] = (lg[0] + lg[1]) + (lg[2] + lg[3])

    def t_copy(i, slot):
        return to_sp(t_src, t_buf.at[slot], t_send.at[i], t_recv.at[slot], NODE * i + q)

    def l_copy(i, slot):
        return to_sp(l_src, l_buf.at[slot], l_send.at[i], l_recv.at[slot], NODE * i + q)

    def send_state(i, _):
        l_copy(i, node).start()
        t_copy(i, node).start()
        return 0

    lax.fori_loop(node + 1, nodes, send_state, 0)

    mark("inner")
    def inside(near_q, near_r, content):
        scores = dot(near_q, near_r, ((1,), (1,)), precision=TOP) * low
        return dot(scores, content, precision=TOP)

    out_w = inside(near_qw, near_rw, v[:, :DV])
    out_n = inside(near_qn, near_rn, v[:, DV:])
    gated = gain_h[...] * silu(gate_in[...].astype(F32))

    sub = iota((n_sp, tokens), 0)
    hit0 = (sub == ids[0:1, :]).astype(F32)
    hit1 = (sub == ids[1:2, :]).astype(F32)
    strict = (iota((tokens, tokens), 0) < iota((tokens, tokens), 1)).astype(BF16)
    taken = dot((hit0 + hit1).astype(BF16), strict)
    row0 = ids[0:1, :].astype(F32) * PADCAP + jnp.sum(taken * hit0, axis=0, keepdims=True)
    row1 = ids[1:2, :].astype(F32) * PADCAP + jnp.sum((taken + hit0) * hit1, axis=0, keepdims=True)

    def upright(row):
        return jnp.broadcast_to(row, (tokens, tokens)).T[:, 0:1]

    pos0, pos1, weight0, weight1 = upright(row0), upright(row1), upright(rw[0:1, :]), upright(rw[1:2, :])
    slot = iota((padded, tokens), 0).astype(F32)
    pick = ((slot == row0) | (slot == row1)).astype(BF16)
    column = iota((tokens, padded), 1).astype(F32)
    weigh = jnp.where(column == pos0, weight0, 0.0) + jnp.where(column == pos1, weight1, 0.0)
    weigh_hi = weigh.astype(BF16)
    weigh_lo = (weigh - weigh_hi.astype(F32)).astype(BF16)
    filled = iota((slots, padded), 0).astype(F32)
    filled = filled + (PADCAP - CAP) * jnp.floor((filled + 0.5) * (1.0 / CAP))
    squeeze = (filled == iota((slots, padded), 1).astype(F32)).astype(BF16)
    spread = iota((padded, slots), 1).astype(F32)
    spread = spread + (PADCAP - CAP) * jnp.floor((spread + 0.5) * (1.0 / CAP))
    spread = (spread == iota((padded, slots), 0).astype(F32)).astype(BF16)

    mark("fold")
    def fold(i, carry):
        l_copy(i, i).wait_recv()
        t_copy(i, i).wait_recv()
        return decay(l_buf[i]) * carry + t_buf[i].astype(F32)

    carry = lax.fori_loop(0, node, fold, jnp.zeros((PART, 128), F32))
    for j in range(NODE):
        x_src[j] = carry
        if j + 1 < NODE:
            carry = decays[j] * carry + st_in[j]
    for i in range(1, NODE):
        x_copy(i, mate(i), q).start()
    x_in[q] = x_src[q]
    mark("xwait")
    for i in range(1, NODE):
        x_copy(i, mate(i), mate(i)).wait_recv()
    mark("mix")
    before = jnp.concatenate([x_in[j] for j in range(NODE)], axis=0)
    in_w = before[:DV]
    in_n = before[DV:]
    in_n = jnp.concatenate([in_n[:, :DKN], in_n[:, DKN:]], axis=0)
    out_w = out_w + dot(far_qw, in_w, ((1,), (1,)), precision=TOP)
    out_n = out_n + dot(far_qn, in_n, ((1,), (1,)), precision=TOP)

    def normed(o):
        return o * lax.rsqrt(jnp.mean(o * o, axis=1, keepdims=True) + EPS)

    mix[p] = (jnp.concatenate([normed(out_w), normed(out_n)], axis=1) * gated).astype(BF16)

    def send_mix(i, _):
        to_tp(mix.at[p], mix.at[p], mix_send.at[i], mix_recv.at[p], lax.rem(p + i, n_tp)).start()
        return 0

    lax.fori_loop(1, n_tp, send_mix, 0)
    mark("project")
    loads[0].wait()

    def w_out_rows(s):
        return wo_v[pl.ds(pl.multiple_of(s * 128, 128), 128), :]

    def project(i, total):
        s = lax.rem(p + n_tp - i, n_tp)
        to_tp(mix.at[s], mix.at[s], mix_send.at[i], mix_recv.at[s], s).wait_recv()
        return total + dot(mix[s], w_out_rows(s))

    projected = lax.fori_loop(1, n_tp, project, dot(mix[p], w_out_rows(p)))
    mark("pack")
    mid = (res[...].astype(F32) + projected).astype(BF16)

    packed = dot(pick, mid).astype(BF16)
    disp_src[...] = packed.reshape(n_sp, PADCAP, 128)
    disp[b] = disp_src[b]

    used = pl.ds(0, CAP)

    def disp_copy(i, src, dst, who):
        return to_sp(disp_src.at[src, used], disp.at[dst, used], disp_send.at[i], disp_recv.at[dst], who)

    def ret_copy(i, src, dst, who):
        return to_sp(ret_src.at[src, used], ret.at[dst, used], ret_send.at[i], ret_recv.at[dst], who)

    def outward(i):
        step = lax.div(i + 1, 2)
        return lax.rem(n_sp // 2 + n_sp + b + step - (2 * step) * lax.rem(i, 2), n_sp)

    def send_rows(i, _):
        who = outward(i)
        disp_copy(i, who, b, who).start()
        return 0

    lax.fori_loop(0, n_sp - 1, send_rows, 0)

    def have_rows(i, _):
        s = lax.rem(b + i, n_sp)
        disp_copy(i, s, s, s).wait_recv()
        return 0

    mark("dispwait")
    lax.fori_loop(1, n_sp, have_rows, 0)
    mark("squeeze")
    rows[p] = dot(squeeze, disp[...].reshape(padded, 128)).astype(BF16)

    side = 4
    half, part = slots // 2, slots // 4
    x, y = lax.rem(p, side), lax.div(p, side)
    spots = ((x, y), (y, x))
    sent = []

    def near(v, step):
        return lax.rem(v + side + step, side)

    def place(plan, f, s):
        return s * side + f if plan == 0 else f * side + s

    def piece(plan, src, which):
        start, size = {"all": (0, half), "lo": (0, part), "hi": (part, part)}[which]
        return rows.at[src, pl.ds(plan * half + start, size)]

    def push(plan, src, which, who):
        at, k = piece(plan, src, which), sum(1 for q, _ in sent if q == plan)
        copy = to_tp(at, at, rows_send.at[plan, k], rows_recv.at[plan, src, int(which == "hi")], who)
        copy.start()
        sent.append((plan, copy))

    def arrive(plan, src, which):
        at, other = piece(plan, src, which), lax.rem(p + 1, n_tp)
        to_tp(at, at, rows_send.at[plan, 0], rows_recv.at[plan, src, int(which == "hi")], other).wait_recv()

    def gate_up(plan, src):
        at = pl.ds(plan * half, half)
        x_in_half = rows[src, at].astype(F32)
        content = (x_in_half * gains[src][0:1]).astype(BF16)
        acc[at, :] += dot(content, wgu[pl.ds(pl.multiple_of(src * 128, 128), 128), :])
        squares[at, :] += x_in_half * x_in_half

    plans = [(plan, f, s) for plan, (f, s) in enumerate(spots)]
    for plan, f, s in plans:
        for who in (place(plan, near(f, 1), s), place(plan, near(f, -1), s), place(plan, f, near(s, 1)), place(plan, f, near(s, -1))):
            push(plan, p, "all", who)
    mark("agown")

    def have_gain(i, _):
        s = lax.rem(p + i, n_tp)
        to_tp(gains.at[s], gains.at[s], gain_send.at[i], gain_recv.at[s], s).wait_recv()
        return 0

    lax.fori_loop(1, n_tp, have_gain, 0)
    for load in loads[1:]:
        load.wait()
    acc[...] = jnp.zeros_like(acc)
    squares[...] = jnp.zeros_like(squares)
    for plan, f, s in plans:
        gate_up(plan, p)
    mark("ag1")
    for plan, f, s in plans:
        for step, which in ((-1, "lo"), (1, "hi")):
            src = place(plan, near(f, step), s)
            arrive(plan, src, "all")
            push(plan, src, which, place(plan, near(f, -step), s))
            push(plan, src, "all", place(plan, f, near(s, 1)))
            push(plan, src, "all", place(plan, f, near(s, -1)))
    mark("ag2")

    def pass_on(plan, f, f_from, s):
        for step, which in ((-1, "lo"), (1, "hi")):
            src = place(plan, f_from, near(s, step))
            arrive(plan, src, "all")
            push(plan, src, which, place(plan, f, near(s, -step)))

    def use(plan, f_from, s_from):
        gate_up(plan, place(plan, f_from, s_from))

    for plan, f, s in plans:
        pass_on(plan, f, f, s)
    for plan, f, s in plans:
        for step in (-1, 1):
            use(plan, near(f, step), s)
    mark("ag3")
    for plan, f, s in plans:
        src = place(plan, near(f, 2), s)
        arrive(plan, src, "lo")
        arrive(plan, src, "hi")
        push(plan, src, "all", place(plan, f, near(s, 1)))
        push(plan, src, "all", place(plan, f, near(s, -1)))
    for plan, f, s in plans:
        for step in (-1, 1):
            use(plan, f, near(s, step))
    mark("ag4")
    for plan, f, s in plans:
        pass_on(plan, f, near(f, -1), s)
        pass_on(plan, f, near(f, 1), s)
    for plan, f, s in plans:
        use(plan, near(f, 2), s)
        for step in (-1, 1):
            use(plan, near(f, -1), near(s, step))
    mark("ag5")
    for plan, f, s in plans:
        pass_on(plan, f, near(f, 2), s)
    for plan, f, s in plans:
        for step in (-1, 1):
            use(plan, near(f, 1), near(s, step))
            use(plan, near(f, 2), near(s, step))
    mark("ag6")
    for step in (0, -1, 1, 2):
        for plan, f, s in plans:
            src = place(plan, near(f, step), near(s, 2))
            arrive(plan, src, "lo")
            arrive(plan, src, "hi")
            gate_up(plan, src)
    mark("act")
    scale = lax.rsqrt(jnp.sum(squares[...], axis=1, keepdims=True) * (1.0 / D) + EPS)
    hidden = (silu(acc[:, :hidden_units] * scale) * (acc[:, hidden_units:] * scale)).astype(BF16)
    mark("down")

    def partial(plan, f, s):
        right = jnp.concatenate([wd_v[place(plan, f, k)] for k in range(side)], axis=1)
        return dot(hidden[plan * half : (plan + 1) * half], right)

    def blocks(value):
        return [[value[q * part : (q + 1) * part, 128 * k : 128 * k + 128] for k in range(side)] for q in range(2)]

    def heavy_copy(plan, way, kind, who):
        return to_tp(
            heavy_src.at[plan, way, kind], heavy.at[plan, way, kind],
            heavy_send.at[plan, way, kind], heavy_recv.at[plan, way, kind], who,
        )

    def light_copy(plan, f, s, step):
        at = plan, step - 1
        return to_tp(
            light_src.at[at], light.at[at], light_send.at[at], light_recv.at[at], place(plan, f, near(s, step)),
        )

    ways = ((0, 1), (1, -1))
    for plan, f, s in plans:
        far = blocks(partial(plan, near(f, 2), s))
        for way, step in ways:
            for k in range(side):
                heavy_src[plan, way, 0, k] = far[way][k].astype(BF16)
            heavy_copy(plan, way, 0, place(plan, near(f, step), s)).start()
    for plan, f, s in plans:
        for way, step in ways:
            next_to = blocks(partial(plan, near(f, step), s))
            for k in range(side):
                heavy_src[plan, way, 1, k] = next_to[1 - way][k].astype(BF16)
                keep[plan, way, k] = next_to[way][k]
            heavy_copy(plan, way, 1, place(plan, near(f, step), s)).start()
    for plan, f, s in plans:
        own = blocks(partial(plan, f, s))
        for q in range(2):
            for k in range(side):
                line[plan, q, k] = own[q][k]
    mark("rs1")
    for plan, f, s in plans:
        for way, step in ways:
            heavy_copy(plan, way, 0, place(plan, near(f, step), s)).wait_recv()
            heavy_src[plan, way, 2] = (keep[plan, way] + heavy[plan, way, 0].astype(F32)).astype(BF16)
            heavy_copy(plan, way, 2, place(plan, near(f, step), s)).start()
    mark("rs2")
    for plan, f, s in plans:
        for way, step in ways:
            heavy_copy(plan, way, 1, place(plan, near(f, step), s)).wait_recv()
            line[plan, 1 - way] += heavy[plan, way, 1].astype(F32)
    mark("rs3")
    for plan, f, s in plans:
        for way, step in ways:
            heavy_copy(plan, way, 2, place(plan, near(f, step), s)).wait_recv()
            line[plan, way] += heavy[plan, way, 2].astype(F32)
        for step in (2, 1, 3):
            for k in range(2):
                light_src[plan, step - 1, k] = line[plan, k, near(s, step)].astype(BF16)
            light_copy(plan, f, s, step).start()
    mark("rs4")
    sums = []
    for plan, f, s in plans:
        value = [line[plan, k, s] for k in range(2)]
        for step in (1, 3, 2):
            light_copy(plan, f, s, step).wait_recv()
            value = [value[k] + light[plan, step - 1, k].astype(F32) for k in range(2)]
        sums += value
    total = jnp.concatenate(sums, axis=0).astype(BF16)

    mark("retsend")
    ret_src[...] = dot(spread, total).astype(BF16).reshape(n_sp, PADCAP, 128)
    ret[b] = ret_src[b]

    def send_back(i, _):
        who = outward(i)
        ret_copy(i, who, b, who).start()
        return 0

    lax.fori_loop(0, n_sp - 1, send_back, 0)

    for i in range(1, NODE):
        st_copy(i, mate(i), q).wait_send()
        lg_copy(i, mate(i), q).wait_send()
        x_copy(i, mate(i), q).wait_send()

    def state_gone(i, _):
        t_copy(i, node).wait_send()
        l_copy(i, node).wait_send()
        return 0

    lax.fori_loop(node + 1, nodes, state_gone, 0)

    def tp_gone(i, _):
        who = lax.rem(p + i, n_tp)
        to_tp(gains.at[p], gains.at[p], gain_send.at[i], gain_recv.at[p], who).wait_send()
        to_tp(mix.at[p], mix.at[p], mix_send.at[i], mix_recv.at[p], who).wait_send()
        return 0

    lax.fori_loop(1, n_tp, tp_gone, 0)

    for _, copy in sent:
        copy.wait_send()
    for plan, f, s in plans:
        for way, step in ways:
            for kind in range(3):
                heavy_copy(plan, way, kind, place(plan, near(f, step), s)).wait_send()
        for step in (1, 2, 3):
            light_copy(plan, f, s, step).wait_send()

    def disp_gone(i, _):
        who = outward(i)
        disp_copy(i, who, b, who).wait_send()
        return 0

    lax.fori_loop(0, n_sp - 1, disp_gone, 0)

    def back_gone(i, _):
        who = outward(i)
        ret_copy(i, who, b, who).wait_send()
        return 0

    def have_back(i, _):
        s = lax.rem(b + i, n_sp)
        ret_copy(i, s, s, s).wait_recv()
        return 0

    mark("retwait")
    lax.fori_loop(1, n_sp, have_back, 0)
    mark("final")
    back = ret[...].reshape(padded, 128)
    moe = dot(weigh_hi, back) + dot(weigh_lo, back)
    out[...] = (mid.astype(F32) + moe).astype(BF16)

    mark("sendwait")
    lax.fori_loop(0, n_sp - 1, back_gone, 0)
    mark()


def body(n_sp, n_tp, *args):
    (res, qw, qn, fw, fn, room_w, room_n, val, gate_in, gain_h, w_out, gain_n, ids, rw, w_gate, w_up, w_down) = args
    tokens = res.shape[0]
    hidden = w_gate.shape[2]
    nodes = n_sp // NODE
    slots = n_sp * CAP
    row = lambda a: a.reshape(1, -1)
    hbm = pl.BlockSpec(memory_space=pl.ANY)
    dma = pltpu.SemaphoreType.DMA
    V = pltpu.VMEM
    half, part = slots // 2, slots // 4
    small = [res, qw, qn.T, fw, fn.T, row(room_w), row(room_n), val, gate_in, row(gain_h), row(gain_n), ids.T, rw.T]
    scratch = [
        *[V(a.shape, a.dtype) for a in small], dma((len(small),)),
        V((D, 128), BF16), V((D, 2 * hidden), BF16), V((n_tp, hidden, 128), BF16), dma((3 + n_tp,)),
        V((NODE, PART, 128), F32), V((NODE, PART, 128), F32), dma((NODE,)), dma((NODE,)),
        V((NODE, 2, 128), F32), dma((NODE,)), dma((NODE,)),
        V((PART, 128), BF16), V((nodes, PART, 128), BF16), V((2, 128), F32), V((nodes, 2, 128), F32),
        dma((nodes,)), dma((nodes,)), dma((nodes,)), dma((nodes,)),
        V((NODE, PART, 128), F32), V((NODE, PART, 128), F32), dma((NODE,)), dma((NODE,)),
        V((n_tp, tokens, 128), BF16), dma((n_tp,)), dma((n_tp,)),
        V((n_tp, 8, 128), F32), dma((n_tp,)), dma((n_tp,)),
        V((n_sp, PADCAP, 128), BF16), V((n_sp, PADCAP, 128), BF16), dma((n_sp,)), dma((n_sp,)),
        V((n_tp, slots, 128), BF16), dma((2, 20)), dma((2, n_tp, 2)),
        V((2, 2, 3, 4, part, 128), BF16), V((2, 2, 3, 4, part, 128), BF16), dma((2, 2, 3)), dma((2, 2, 3)),
        V((2, 3, 2, part, 128), BF16), V((2, 3, 2, part, 128), BF16), dma((2, 3)), dma((2, 3)),
        V((2, 2, 4, part, 128), F32), V((2, 2, 4, part, 128), F32),
        V((n_sp, PADCAP, 128), BF16), V((n_sp, PADCAP, 128), BF16), dma((n_sp,)), dma((n_sp,)),
        V((slots, 2 * hidden), F32), V((slots, 128), F32),
    ]
    return pl.pallas_call(
        functools.partial(kernel, n_sp, n_tp, slots),
        out_shape=jax.ShapeDtypeStruct((tokens, 128), BF16),
        in_specs=[hbm] * 17,
        out_specs=pl.BlockSpec(memory_space=pltpu.VMEM),
        scratch_shapes=scratch,
        compiler_params=pltpu.CompilerParams(
            collective_id=0, has_side_effects=True, vmem_limit_bytes=67043328
        ),
    )(*small[:10], w_out, *small[10:], w_gate, w_up, w_down)


def solution(mesh):
    both = P("sp", "tp")
    placed = (
        both, both, both, both, both, P("tp"), P("tp"), both, both, P("tp"), P(None, "tp"), P("tp"),
        P("sp", None), P("sp", None), P("sp", None, "tp"), P("sp", None, "tp"), P("sp", "tp", None),
    )
    fn = functools.partial(body, mesh.shape["sp"], mesh.shape["tp"])
    return jax.shard_map(fn, mesh=mesh, in_specs=placed, out_specs=both, check_vma=False)
```

time: 112 us -> 90 us (0.80)
  Pallas kernels: 104 us -> 88.3 us
  local copies, waits for them, and re-layouts: 7.7 us -> 1.38 us
    pallas_call x1, Pallas kernels: 104 us -> 88.3 us  [body(): pl.pallas_call(functools.partial(kernel, n_sp, n_tp, slots), out_shape=ja...]
    unnamed x37 -> x1, local copies, waits for them, and re-layouts: 7.7 us -> 1.38 us
where the time goes in v2:
time: 90 us; the launch traced here: 89.7 us
  Pallas kernels  88.3 us (98%)
  local copies, waits for them, and re-layouts  1.38 us (2%)
    pallas_call x1, Pallas kernels, body(): pl.pallas_call(functools.partial(kernel, n_sp, n_tp, slots), out_shape=ja...  88.3 us

profile of v2, /device:TPU:1, one launch (start us, length us, event | category | flops | bytes accessed | tf_op | source)
XLA Modules:
  0.0 89.7 jit_solution(16110793759119023982)
XLA Ops:
  0.0 88.3 %shard_map.163 = bf16[128,128]{1,0:T(8,128)(2,1)} custom-call(bf16[128,128]{1,0:T(8,128)(2,1)} %res_h.1, bf16[128,128]{1,0:T(8,128)(2,1)} %qw_h.1, bf16[64,128]{1,0:T(8,128)(2,1)} %bitcast.8, bf16[128,128]{1,0:T(8,128)(2,1)} %fw_h.1, bf16[64,128]{1,0:T(8,128)(2,1)} %bitcast.9, f32[1,128]{1,0:T(1,128)} %bitcast.12, f32[1,64]{1,0:T(1,128)} %bitcast.13, ...), custom_call_target="tpu_custom_call" | custom-call | tf_op jit(solution)/shard_map/pallas_call | solution.py:596
  88.3 1.4 %copy.19 = bf16[128,128]{1,0:T(8,128)(2,1)} copy(bf16[128,128]{1,0:T(8,128)(2,1)} %shard_map.163) | data formatting | bytes 65536

commit v3 on v2

--- a/solution.py
+++ b/solution.py
@@ -115,6 +115,19 @@
     def to_tp(src, dst, send, recv, who):
         return pltpu.make_async_remote_copy(src, dst, send, recv, device_id={"tp": who}, device_id_type=MESH)
 
+    side = 4
+    half, part = slots // 2, slots // 4
+    x, y = lax.rem(p, side), lax.div(p, side)
+    spots = ((x, y), (y, x))
+
+    def near(v, step):
+        return lax.rem(v + side + step, side)
+
+    def place(plan, f, s):
+        return s * side + f if plan == 0 else f * side + s
+
+    plans = [(plan, f, s) for plan, (f, s) in enumerate(spots)]
+
     mark("local")
     low = (iota((tokens, tokens), 0) >= iota((tokens, tokens), 1)).astype(F32)
 
@@ -135,7 +148,7 @@
     s_n = jnp.concatenate([s_n[: DV // 2], s_n[DV // 2 :]], axis=1)
     states = jnp.concatenate([s_w, s_n], axis=0)
     for j in range(NODE):
-        st[j] = states[j * PART : (j + 1) * PART]
+        st[j] = states[j * PART : (j + 1) * PART].astype(BF16)
     lg[q] = jnp.concatenate([end_w, jnp.concatenate([end_n, end_n], axis=1)], axis=0)
 
     mark("barrier")
@@ -178,9 +191,10 @@
         lg_copy(i, mate(i), mate(i)).wait_recv()
         st_copy(i, mate(i), mate(i)).wait_recv()
     decays = [decay(lg[j]) for j in range(NODE)]
-    whole = st_in[0]
+    ends = [st_in[j].astype(F32) for j in range(NODE)]
+    whole = ends[0]
     for j in range(1, NODE):
-        whole = decays[j] * whole + st_in[j]
+        whole = decays[j] * whole + ends[j]
     t_src[...] = whole.astype(BF16)
     l_src[...] = (lg[0] + lg[1]) + (lg[2] + lg[3])
 
@@ -239,9 +253,9 @@
 
     carry = lax.fori_loop(0, node, fold, jnp.zeros((PART, 128), F32))
     for j in range(NODE):
-        x_src[j] = carry
+        x_src[j] = carry.astype(BF16)
         if j + 1 < NODE:
-            carry = decays[j] * carry + st_in[j]
+            carry = decays[j] * carry + ends[j]
     for i in range(1, NODE):
         x_copy(i, mate(i), q).start()
     x_in[q] = x_src[q]
@@ -249,7 +263,7 @@
     for i in range(1, NODE):
         x_copy(i, mate(i), mate(i)).wait_recv()
     mark("mix")
-    before = jnp.concatenate([x_in[j] for j in range(NODE)], axis=0)
+    before = jnp.concatenate([x_in[j].astype(F32) for j in range(NODE)], axis=0)
     in_w = before[:DV]
     in_n = before[DV:]
     in_n = jnp.concatenate([in_n[:, :DKN], in_n[:, DKN:]], axis=0)
@@ -261,23 +275,54 @@
 
     mix[p] = (jnp.concatenate([normed(out_w), normed(out_n)], axis=1) * gated).astype(BF16)
 
-    def send_mix(i, _):
-        to_tp(mix.at[p], mix.at[p], mix_send.at[i], mix_recv.at[p], lax.rem(p + i, n_tp)).start()
-        return 0
-
-    lax.fori_loop(1, n_tp, send_mix, 0)
+    mix_sent = []
+
+    def mix_copy(plan, k, src, who):
+        at = mix.at[src, pl.ds(plan * (tokens // 2), tokens // 2)]
+        return to_tp(at, at, mix_send.at[plan, k], mix_recv.at[plan, src], who)
+
+    def mix_push(plan, src, who):
+        copy = mix_copy(plan, sum(1 for k, _ in mix_sent if k == plan), src, who)
+        copy.start()
+        mix_sent.append((plan, copy))
+
+    def mix_arrive(plan, src):
+        mix_copy(plan, 0, src, lax.rem(p + 1, n_tp)).wait_recv()
+
+    for plan, f, s in plans:
+        for step in (2, 1, -1):
+            mix_push(plan, p, place(plan, near(f, step), s))
+    for plan, f, s in plans:
+        for step in (2, 1, -1):
+            mix_push(plan, p, place(plan, f, near(s, step)))
     mark("project")
+    for step in (1, -1, 2):
+        for plan, f, s in plans:
+            src = place(plan, near(f, step), s)
+            mix_arrive(plan, src)
+            for other in (2, 1, -1):
+                mix_push(plan, src, place(plan, f, near(s, other)))
+    mark("project2")
     loads[0].wait()
 
-    def w_out_rows(s):
-        return wo_v[pl.ds(pl.multiple_of(s * 128, 128), 128), :]
-
-    def project(i, total):
-        s = lax.rem(p + n_tp - i, n_tp)
-        to_tp(mix.at[s], mix.at[s], mix_send.at[i], mix_recv.at[s], s).wait_recv()
-        return total + dot(mix[s], w_out_rows(s))
-
-    projected = lax.fori_loop(1, n_tp, project, dot(mix[p], w_out_rows(p)))
+    def w_out_rows(src):
+        return wo_v[pl.ds(pl.multiple_of(src * 128, 128), 128), :]
+
+    for step in (1, -1, 2):
+        for plan, f, s in plans:
+            mix_arrive(plan, place(plan, f, near(s, step)))
+
+    def project(sources):
+        left = jnp.concatenate([mix[src] for src in sources], axis=1)
+        return dot(left, jnp.concatenate([w_out_rows(src) for src in sources], axis=0))
+
+    projected = project([p] + [y * side + near(x, k) for k in (1, 2, 3)] + [near(y, k) * side + x for k in (1, 2, 3)])
+    mark("project3")
+    for first in (1, -1, 2):
+        for step in (1, -1, 2):
+            for plan, f, s in plans:
+                mix_arrive(plan, place(plan, near(f, first), near(s, step)))
+    projected = projected + project([near(y, k) * side + near(x, j) for k in (1, 2, 3) for j in (1, 2, 3)])
     mark("pack")
     mid = (res[...].astype(F32) + projected).astype(BF16)
 
@@ -293,52 +338,36 @@
     def ret_copy(i, src, dst, who):
         return to_sp(ret_src.at[src, used], ret.at[dst, used], ret_send.at[i], ret_recv.at[dst], who)
 
-    def outward(i):
-        step = lax.div(i + 1, 2)
-        return lax.rem(n_sp // 2 + n_sp + b + step - (2 * step) * lax.rem(i, 2), n_sp)
-
-    def send_rows(i, _):
-        who = outward(i)
+    outward = [lax.rem(b + n_sp // 2, n_sp)]
+    for step in range(1, n_sp // 2):
+        outward += [lax.rem(b + n_sp // 2 + step, n_sp), lax.rem(b + n_sp // 2 - step, n_sp)]
+    for i, who in enumerate(outward):
         disp_copy(i, who, b, who).start()
-        return 0
-
-    lax.fori_loop(0, n_sp - 1, send_rows, 0)
-
-    def have_rows(i, _):
-        s = lax.rem(b + i, n_sp)
-        disp_copy(i, s, s, s).wait_recv()
-        return 0
-
     mark("dispwait")
-    lax.fori_loop(1, n_sp, have_rows, 0)
+    for i, who in enumerate(reversed(outward)):
+        disp_copy(i, who, who, who).wait_recv()
     mark("squeeze")
     rows[p] = dot(squeeze, disp[...].reshape(padded, 128)).astype(BF16)
 
-    side = 4
-    half, part = slots // 2, slots // 4
-    x, y = lax.rem(p, side), lax.div(p, side)
-    spots = ((x, y), (y, x))
     sent = []
 
-    def near(v, step):
-        return lax.rem(v + side + step, side)
-
-    def place(plan, f, s):
-        return s * side + f if plan == 0 else f * side + s
-
-    def piece(plan, src, which):
-        start, size = {"all": (0, half), "lo": (0, part), "hi": (part, part)}[which]
-        return rows.at[src, pl.ds(plan * half + start, size)]
-
-    def push(plan, src, which, who):
-        at, k = piece(plan, src, which), sum(1 for q, _ in sent if q == plan)
-        copy = to_tp(at, at, rows_send.at[plan, k], rows_recv.at[plan, src, int(which == "hi")], who)
+    def row_copy(plan, k, src, q, who):
+        at = rows.at[src, pl.ds(plan * half + q * part, part)]
+        return to_tp(at, at, rows_send.at[plan, k], rows_recv.at[plan, src, q], who)
+
+    def push(plan, src, q, who):
+        copy = row_copy(plan, sum(1 for k, _ in sent if k == plan), src, q, who)
         copy.start()
         sent.append((plan, copy))
 
-    def arrive(plan, src, which):
-        at, other = piece(plan, src, which), lax.rem(p + 1, n_tp)
-        to_tp(at, at, rows_send.at[plan, 0], rows_recv.at[plan, src, int(which == "hi")], other).wait_recv()
+    def arrive(plan, src, q):
+        row_copy(plan, 0, src, q, lax.rem(p + 1, n_tp)).wait_recv()
+
+    def push_both(plan, src, ahead, behind):
+        push(plan, src, 0, ahead)
+        push(plan, src, 1, behind)
+        push(plan, src, 1, ahead)
+        push(plan, src, 0, behind)
 
     def gate_up(plan, src):
         at = pl.ds(plan * half, half)
@@ -347,10 +376,10 @@
         acc[at, :] += dot(content, wgu[pl.ds(pl.multiple_of(src * 128, 128), 128), :])
         squares[at, :] += x_in_half * x_in_half
 
-    plans = [(plan, f, s) for plan, (f, s) in enumerate(spots)]
-    for plan, f, s in plans:
-        for who in (place(plan, near(f, 1), s), place(plan, near(f, -1), s), place(plan, f, near(s, 1)), place(plan, f, near(s, -1))):
-            push(plan, p, "all", who)
+    for plan, f, s in plans:
+        push_both(plan, p, place(plan, near(f, 1), s), place(plan, near(f, -1), s))
+    for plan, f, s in plans:
+        push_both(plan, p, place(plan, f, near(s, 1)), place(plan, f, near(s, -1)))
     mark("agown")
 
     def have_gain(i, _):
@@ -367,130 +396,132 @@
         gate_up(plan, p)
     mark("ag1")
     for plan, f, s in plans:
-        for step, which in ((-1, "lo"), (1, "hi")):
+        for q, step in ((0, -1), (1, 1)):
             src = place(plan, near(f, step), s)
-            arrive(plan, src, "all")
-            push(plan, src, which, place(plan, near(f, -step), s))
-            push(plan, src, "all", place(plan, f, near(s, 1)))
-            push(plan, src, "all", place(plan, f, near(s, -1)))
+            arrive(plan, src, q)
+            push(plan, src, q, place(plan, near(f, -step), s))
+    for plan, f, s in plans:
+        for q, step in ((0, -1), (1, 1)):
+            src = place(plan, near(f, step), s)
+            arrive(plan, src, 1 - q)
+            push_both(plan, src, place(plan, f, near(s, 1)), place(plan, f, near(s, -1)))
     mark("ag2")
 
     def pass_on(plan, f, f_from, s):
-        for step, which in ((-1, "lo"), (1, "hi")):
+        for q, step in ((0, -1), (1, 1)):
             src = place(plan, f_from, near(s, step))
-            arrive(plan, src, "all")
-            push(plan, src, which, place(plan, f, near(s, -step)))
-
-    def use(plan, f_from, s_from):
-        gate_up(plan, place(plan, f_from, s_from))
+            arrive(plan, src, q)
+            push(plan, src, q, place(plan, f, near(s, -step)))
+
+    def finish(plan, f_from, s):
+        for q, step in ((0, -1), (1, 1)):
+            arrive(plan, place(plan, f_from, near(s, step)), 1 - q)
+            gate_up(plan, place(plan, f_from, near(s, step)))
 
     for plan, f, s in plans:
         pass_on(plan, f, f, s)
     for plan, f, s in plans:
         for step in (-1, 1):
-            use(plan, near(f, step), s)
+            gate_up(plan, place(plan, near(f, step), s))
     mark("ag3")
-    for plan, f, s in plans:
-        src = place(plan, near(f, 2), s)
-        arrive(plan, src, "lo")
-        arrive(plan, src, "hi")
-        push(plan, src, "all", place(plan, f, near(s, 1)))
-        push(plan, src, "all", place(plan, f, near(s, -1)))
-    for plan, f, s in plans:
-        for step in (-1, 1):
-            use(plan, f, near(s, step))
+    for q in (0, 1):
+        for plan, f, s in plans:
+            src = place(plan, near(f, 2), s)
+            arrive(plan, src, q)
+            step = 1 - 2 * q
+            push(plan, src, q, place(plan, f, near(s, step)))
+            push(plan, src, q, place(plan, f, near(s, -step)))
+    for plan, f, s in plans:
+        finish(plan, f, s)
     mark("ag4")
     for plan, f, s in plans:
         pass_on(plan, f, near(f, -1), s)
         pass_on(plan, f, near(f, 1), s)
     for plan, f, s in plans:
-        use(plan, near(f, 2), s)
-        for step in (-1, 1):
-            use(plan, near(f, -1), near(s, step))
+        gate_up(plan, place(plan, near(f, 2), s))
+        finish(plan, near(f, -1), s)
     mark("ag5")
     for plan, f, s in plans:
         pass_on(plan, f, near(f, 2), s)
     for plan, f, s in plans:
-        for step in (-1, 1):
-            use(plan, near(f, 1), near(s, step))
-            use(plan, near(f, 2), near(s, step))
+        finish(plan, near(f, 1), s)
+        finish(plan, near(f, 2), s)
     mark("ag6")
     for step in (0, -1, 1, 2):
         for plan, f, s in plans:
             src = place(plan, near(f, step), near(s, 2))
-            arrive(plan, src, "lo")
-            arrive(plan, src, "hi")
+            arrive(plan, src, 0)
+            arrive(plan, src, 1)
             gate_up(plan, src)
     mark("act")
     scale = lax.rsqrt(jnp.sum(squares[...], axis=1, keepdims=True) * (1.0 / D) + EPS)
     hidden = (silu(acc[:, :hidden_units] * scale) * (acc[:, hidden_units:] * scale)).astype(BF16)
     mark("down")
 
+    order = (2, 1, 3, 0)
+
     def partial(plan, f, s):
-        right = jnp.concatenate([wd_v[place(plan, f, k)] for k in range(side)], axis=1)
-        return dot(hidden[plan * half : (plan + 1) * half], right)
-
-    def blocks(value):
+        right = jnp.concatenate([wd_v[place(plan, f, near(s, r))] for r in order], axis=1)
+        value = dot(hidden[plan * half : (plan + 1) * half], right)
         return [[value[q * part : (q + 1) * part, 128 * k : 128 * k + 128] for k in range(side)] for q in range(2)]
 
-    def heavy_copy(plan, way, kind, who):
-        return to_tp(
-            heavy_src.at[plan, way, kind], heavy.at[plan, way, kind],
-            heavy_send.at[plan, way, kind], heavy_recv.at[plan, way, kind], who,
-        )
-
-    def light_copy(plan, f, s, step):
-        at = plan, step - 1
-        return to_tp(
-            light_src.at[at], light.at[at], light_send.at[at], light_recv.at[at], place(plan, f, near(s, step)),
-        )
-
-    ways = ((0, 1), (1, -1))
-    for plan, f, s in plans:
-        far = blocks(partial(plan, near(f, 2), s))
-        for way, step in ways:
+    def heavy_copy(plan, way, kind, k):
+        at = plan, way, kind, k
+        _, f, s = plans[plan]
+        who = place(plan, near(f, 1 - 2 * way), s)
+        return to_tp(heavy_src.at[at], heavy.at[at], heavy_send.at[at], heavy_recv.at[at], who)
+
+    def light_copy(plan, k):
+        at = plan, k
+        _, f, s = plans[plan]
+        who = place(plan, f, near(s, order[k]))
+        return to_tp(light_src.at[at], light.at[at], light_send.at[at], light_recv.at[at], who)
+
+    both = [(plan, way) for plan in range(2) for way in range(2)]
+    for plan, f, s in plans:
+        far = partial(plan, near(f, 2), s)
+        for k in range(side):
+            for way in range(2):
+                heavy_src[plan, way, 0, k] = far[way][k].astype(BF16)
+                heavy_copy(plan, way, 0, k).start()
+    for plan, f, s in plans:
+        for way in range(2):
+            beside = partial(plan, near(f, 1 - 2 * way), s)
             for k in range(side):
-                heavy_src[plan, way, 0, k] = far[way][k].astype(BF16)
-            heavy_copy(plan, way, 0, place(plan, near(f, step), s)).start()
-    for plan, f, s in plans:
-        for way, step in ways:
-            next_to = blocks(partial(plan, near(f, step), s))
-            for k in range(side):
-                heavy_src[plan, way, 1, k] = next_to[1 - way][k].astype(BF16)
-                keep[plan, way, k] = next_to[way][k]
-            heavy_copy(plan, way, 1, place(plan, near(f, step), s)).start()
-    for plan, f, s in plans:
-        own = blocks(partial(plan, f, s))
+                heavy_src[plan, way, 1, k] = beside[1 - way][k].astype(BF16)
+                heavy_copy(plan, way, 1, k).start()
+                keep[plan, way, k] = beside[way][k]
+    for plan, f, s in plans:
+        own = partial(plan, f, s)
         for q in range(2):
             for k in range(side):
                 line[plan, q, k] = own[q][k]
     mark("rs1")
-    for plan, f, s in plans:
-        for way, step in ways:
-            heavy_copy(plan, way, 0, place(plan, near(f, step), s)).wait_recv()
-            heavy_src[plan, way, 2] = (keep[plan, way] + heavy[plan, way, 0].astype(F32)).astype(BF16)
-            heavy_copy(plan, way, 2, place(plan, near(f, step), s)).start()
+    for k in range(side):
+        for plan, way in both:
+            heavy_copy(plan, way, 0, k).wait_recv()
+            heavy_src[plan, way, 2, k] = (keep[plan, way, k] + heavy[plan, way, 0, k].astype(F32)).astype(BF16)
+            heavy_copy(plan, way, 2, k).start()
     mark("rs2")
-    for plan, f, s in plans:
-        for way, step in ways:
-            heavy_copy(plan, way, 1, place(plan, near(f, step), s)).wait_recv()
-            line[plan, 1 - way] += heavy[plan, way, 1].astype(F32)
+    for k in range(side):
+        for plan, way in both:
+            heavy_copy(plan, way, 1, k).wait_recv()
+            line[plan, 1 - way, k] += heavy[plan, way, 1, k].astype(F32)
     mark("rs3")
-    for plan, f, s in plans:
-        for way, step in ways:
-            heavy_copy(plan, way, 2, place(plan, near(f, step), s)).wait_recv()
-            line[plan, way] += heavy[plan, way, 2].astype(F32)
-        for step in (2, 1, 3):
-            for k in range(2):
-                light_src[plan, step - 1, k] = line[plan, k, near(s, step)].astype(BF16)
-            light_copy(plan, f, s, step).start()
+    for k in range(side):
+        for plan, way in both:
+            heavy_copy(plan, way, 2, k).wait_recv()
+            line[plan, way, k] += heavy[plan, way, 2, k].astype(F32)
+            if k < 3 and way == 1:
+                light_src[plan, k] = line[plan, :, k].astype(BF16)
+                light_copy(plan, k).start()
     mark("rs4")
     sums = []
-    for plan, f, s in plans:
-        value = [line[plan, k, s] for k in range(2)]
-        for step in (1, 3, 2):
-            light_copy(plan, f, s, step).wait_recv()
-            value = [value[k] + light[plan, step - 1, k].astype(F32) for k in range(2)]
+    for plan in range(2):
+        value = [line[plan, q, 3] for q in range(2)]
+        for k in (1, 2, 0):
+            light_copy(plan, k).wait_recv()
+            value = [value[q] + light[plan, k, q].astype(F32) for q in range(2)]
         sums += value
     total = jnp.concatenate(sums, axis=0).astype(BF16)
 
@@ -498,13 +529,9 @@
     ret_src[...] = dot(spread, total).astype(BF16).reshape(n_sp, PADCAP, 128)
     ret[b] = ret_src[b]
 
-    def send_back(i, _):
-        who = outward(i)
+    for i, who in enumerate(outward):
         ret_copy(i, who, b, who).start()
-        return 0
-
-    lax.fori_loop(0, n_sp - 1, send_back, 0)
-
+    mark("retwait")
     for i in range(1, NODE):
         st_copy(i, mate(i), q).wait_send()
         lg_copy(i, mate(i), q).wait_send()
@@ -520,46 +547,32 @@
     def tp_gone(i, _):
         who = lax.rem(p + i, n_tp)
         to_tp(gains.at[p], gains.at[p], gain_send.at[i], gain_recv.at[p], who).wait_send()
-        to_tp(mix.at[p], mix.at[p], mix_send.at[i], mix_recv.at[p], who).wait_send()
         return 0
 
     lax.fori_loop(1, n_tp, tp_gone, 0)
 
-    for _, copy in sent:
+    for _, copy in mix_sent + sent:
         copy.wait_send()
-    for plan, f, s in plans:
-        for way, step in ways:
-            for kind in range(3):
-                heavy_copy(plan, way, kind, place(plan, near(f, step), s)).wait_send()
-        for step in (1, 2, 3):
-            light_copy(plan, f, s, step).wait_send()
-
-    def disp_gone(i, _):
-        who = outward(i)
+    for plan in range(2):
+        for k in range(side):
+            for way in range(2):
+                for kind in range(3):
+                    heavy_copy(plan, way, kind, k).wait_send()
+            if k < 3:
+                light_copy(plan, k).wait_send()
+    for i, who in enumerate(outward):
         disp_copy(i, who, b, who).wait_send()
-        return 0
-
-    lax.fori_loop(0, n_sp - 1, disp_gone, 0)
-
-    def back_gone(i, _):
-        who = outward(i)
-        ret_copy(i, who, b, who).wait_send()
-        return 0
-
-    def have_back(i, _):
-        s = lax.rem(b + i, n_sp)
-        ret_copy(i, s, s, s).wait_recv()
-        return 0
-
-    mark("retwait")
-    lax.fori_loop(1, n_sp, have_back, 0)
+    mark("retwait2")
+    for i, who in enumerate(reversed(outward)):
+        ret_copy(i, who, who, who).wait_recv()
     mark("final")
     back = ret[...].reshape(padded, 128)
     moe = dot(weigh_hi, back) + dot(weigh_lo, back)
     out[...] = (mid.astype(F32) + moe).astype(BF16)
 
     mark("sendwait")
-    lax.fori_loop(0, n_sp - 1, back_gone, 0)
+    for i, who in enumerate(outward):
+        ret_copy(i, who, b, who).wait_send()
     mark()
 
 
@@ -578,16 +591,16 @@
     scratch = [
         *[V(a.shape, a.dtype) for a in small], dma((len(small),)),
         V((D, 128), BF16), V((D, 2 * hidden), BF16), V((n_tp, hidden, 128), BF16), dma((3 + n_tp,)),
-        V((NODE, PART, 128), F32), V((NODE, PART, 128), F32), dma((NODE,)), dma((NODE,)),
+        V((NODE, PART, 128), BF16), V((NODE, PART, 128), BF16), dma((NODE,)), dma((NODE,)),
         V((NODE, 2, 128), F32), dma((NODE,)), dma((NODE,)),
         V((PART, 128), BF16), V((nodes, PART, 128), BF16), V((2, 128), F32), V((nodes, 2, 128), F32),
         dma((nodes,)), dma((nodes,)), dma((nodes,)), dma((nodes,)),
-        V((NODE, PART, 128), F32), V((NODE, PART, 128), F32), dma((NODE,)), dma((NODE,)),
-        V((n_tp, tokens, 128), BF16), dma((n_tp,)), dma((n_tp,)),
+        V((NODE, PART, 128), BF16), V((NODE, PART, 128), BF16), dma((NODE,)), dma((NODE,)),
+        V((n_tp, tokens, 128), BF16), dma((2, n_tp)), dma((2, n_tp)),
         V((n_tp, 8, 128), F32), dma((n_tp,)), dma((n_tp,)),
         V((n_sp, PADCAP, 128), BF16), V((n_sp, PADCAP, 128), BF16), dma((n_sp,)), dma((n_sp,)),
-        V((n_tp, slots, 128), BF16), dma((2, 20)), dma((2, n_tp, 2)),
-        V((2, 2, 3, 4, part, 128), BF16), V((2, 2, 3, 4, part, 128), BF16), dma((2, 2, 3)), dma((2, 2, 3)),
+        V((n_tp, slots, 128), BF16), dma((2, 30)), dma((2, n_tp, 2)),
+        V((2, 2, 3, 4, part, 128), BF16), V((2, 2, 3, 4, part, 128), BF16), dma((2, 2, 3, 4)), dma((2, 2, 3, 4)),
         V((2, 3, 2, part, 128), BF16), V((2, 3, 2, part, 128), BF16), dma((2, 3)), dma((2, 3)),
         V((2, 2, 4, part, 128), F32), V((2, 2, 4, part, 128), F32),
         V((n_sp, PADCAP, 128), BF16), V((n_sp, PADCAP, 128), BF16), dma((n_sp,)), dma((n_sp,)),

time: 90 us -> 85.5 us (0.950)
  Pallas kernels: 88.3 us -> 83.9 us
    pallas_call x1, Pallas kernels: 88.3 us -> 83.9 us  [body(): pl.pallas_call(functools.partial(kernel, n_sp, n_tp, slots), out_shape=ja...]
where the time goes in v3:
time: 85.5 us; the launch traced here: 85.3 us
  Pallas kernels  83.9 us (98%)
  local copies, waits for them, and re-layouts  1.38 us (2%)
    pallas_call x1, Pallas kernels, body(): pl.pallas_call(functools.partial(kernel, n_sp, n_tp, slots), out_shape=ja...  83.9 us

profile of v3, /device:TPU:1, one launch (start us, length us, event | category | flops | bytes accessed | tf_op | source)
XLA Modules:
  0.0 85.3 jit_solution(4416143975531192297)
XLA Ops:
  0.0 83.9 %shard_map.163 = bf16[128,128]{1,0:T(8,128)(2,1)} custom-call(bf16[128,128]{1,0:T(8,128)(2,1)} %res_h.1, bf16[128,128]{1,0:T(8,128)(2,1)} %qw_h.1, bf16[64,128]{1,0:T(8,128)(2,1)} %bitcast.8, bf16[128,128]{1,0:T(8,128)(2,1)} %fw_h.1, bf16[64,128]{1,0:T(8,128)(2,1)} %bitcast.9, f32[1,128]{1,0:T(1,128)} %bitcast.12, f32[1,64]{1,0:T(1,128)} %bitcast.13, ...), custom_call_target="tpu_custom_call" | custom-call | tf_op jit(solution)/shard_map/pallas_call | solution.py:609
  83.9 1.4 %copy.19 = bf16[128,128]{1,0:T(8,128)(2,1)} copy(bf16[128,128]{1,0:T(8,128)(2,1)} %shard_map.163) | data formatting | bytes 65536
